TPU v7x, 512 devices: a whole 4x4x16 slice. The times are simulated.
512 devices in a mesh: ep: 32 (over z, core), tp: 16 (over y, x).
Axes of the slice: x: 4, y: 4, z: 16, core: 2. Of those that a mesh axis runs over, the one named last changes fastest.
Arguments:
- tokens: bfloat16 [4096, 2048], P('ep'), may hold values from -6 to 6
- routes: int32 [4096, 2], P('ep'), may hold values from 0 to 15, all different within a row; in each aligned block of 128 rows (0 to 127, 128 to 255, ...) at most 18 rows name the same one
- route_weights: float32 [4096, 2], P('ep'), may hold values from 0.2 to 1
- out_grad: bfloat16 [4096, 2048], P('ep'), may hold values from -6 to 6
- gate_proj: bfloat16 [32, 2048, 2048], P('ep', None, 'tp'), may hold values from -0.125 to 0.125
- up_proj: bfloat16 [32, 2048, 2048], P('ep', None, 'tp'), may hold values from -0.125 to 0.125
- down_proj: bfloat16 [32, 2048, 2048], P('ep', 'tp'), may hold values from -0.09375 to 0.09375
Outputs:
- tokens_grad: bfloat16 [4096, 2048], P('ep', 'tp')
- route_grad: float32 [4096, 2], P('ep')
- gate_grad: bfloat16 [32, 2048, 2048], P('ep', None, 'tp')
- up_grad: bfloat16 [32, 2048, 2048], P('ep', None, 'tp')
- down_grad: bfloat16 [32, 2048, 2048], P('ep', 'tp')
Inputs may be any that keep to these rules, and one draw needn't show every extreme that they name: `routes`: each row names 2 different experts. In the rows of one device (an aligned block of 128 rows) no expert is named more than 18 times, and in some blocks one expert is named exactly 18 times.
All inputs are finite; a program needn't handle non-finite values.
Results may differ from a plain program's by a relative error of at most 0.019.
Values may be sent and summed in bfloat16 or wider, within the bound.
A program may use at most 64 MiB of HBM per device.

v0:
```python
import jax
import jax.numpy as jnp
from jax import lax
from jax.sharding import Mesh
from jax.sharding import PartitionSpec as P

EP = ("ep_0", "ep_1")


def cut_along(array, dim, length):
    before, after = (array.shape[:dim], array.shape[dim + 1 :])
    return jnp.moveaxis(array.reshape(*before, length, -1, *after), dim, 0)


def joined_along(pieces, dim):
    shape = list(pieces.shape[1:])
    shape[dim] *= pieces.shape[0]
    return jnp.moveaxis(pieces, 0, dim).reshape(shape)


def moved_by_axis(pieces, axes, sequence):
    inside = pieces.shape[1:]
    result = pieces.reshape(*(lax.axis_size(a) for a in axes), *inside)
    for k in sequence:
        result = lax.all_to_all(result, axes[k], k, k, tiled=True)
    return result.reshape(-1, *inside)


def two_step_exchange(array, groups, sequence, split_dim, concat_dim):
    length = lax.axis_size(groups[0]) * lax.axis_size(groups[1])
    pieces = cut_along(array, split_dim, length)
    return joined_along(moved_by_axis(pieces, groups, sequence), concat_dim)


def for_sending(array):

    def short(part):
        return part.astype(jnp.bfloat16) if part.dtype == jnp.float32 else part

    return jax.tree.map(short, array)


def partner_2(array, axis, apart):
    return lax.ppermute(array, axis, [(i, i ^ 1 << apart) for i in range(lax.axis_size(axis))])


def side_by_side(arrays, axis, dim, along):
    widths = [a.shape[along] for a in arrays]
    both = jnp.concatenate(arrays, axis=along)
    result = lax.all_gather(both, axis, axis=dim, tiled=True)
    return tuple(jnp.split(result, [sum(widths[:k]) for k in range(1, len(widths))], axis=along))


def sum_at_owner(array, axis, dim):
    length = lax.axis_size(axis)
    pieces = lax.all_to_all(cut_along(array, dim, length), axis, 0, 0, tiled=True)
    return jnp.sum(pieces.astype(jnp.float32), axis=0)


def copy_for_each(array, axis):
    copies = jnp.broadcast_to(array, (lax.axis_size(axis), *array.shape))
    return lax.all_to_all(copies, axis, split_axis=0, concat_axis=0, tiled=True)


def over_copies(array, axis):
    everything = copy_for_each(array, axis)
    return jnp.sum(everything, axis=0)


def slot_rows(routes, expert_count, capacity):
    flat_routes = routes.reshape(-1)
    one_hot = (flat_routes[:, None] == jnp.arange(expert_count, dtype=jnp.int32)[None, :]).astype(
        jnp.int32
    )
    earlier = jnp.cumsum(one_hot, axis=0) - one_hot
    slot_index = jnp.sum(earlier * one_hot, axis=1)
    return flat_routes * capacity + slot_index


def contract_rows(left, right):
    return lax.dot_general(
        left, right, (((0,), (0,)), ((), ())), preferred_element_type=jnp.float32
    )


def contract_cols(left, right):
    return lax.dot_general(
        left, right, (((1,), (1,)), ((), ())), preferred_element_type=jnp.float32
    )


def local(tokens, routes, route_weights, out_grad, gate_proj, up_proj, down_proj):
    ep_size = lax.axis_size(EP)
    expert_count = ep_size // 2
    token_count, model_width = tokens.shape
    top_count = routes.shape[1]
    capacity = 9 * token_count * top_count // (8 * expert_count)
    slot_count = expert_count * capacity
    col_width = model_width // lax.axis_size("tp")
    col_start = lax.axis_index("tp") * col_width
    destination = slot_rows(routes, expert_count, capacity)
    pair_ids = jnp.arange(token_count * top_count, dtype=jnp.int32)
    slot_source = jnp.zeros((slot_count,), jnp.int32).at[destination].set(pair_ids)
    used = jnp.zeros((slot_count,), jnp.bool_).at[destination].set(True)
    token_ids = slot_source // top_count
    token_cols = lax.dynamic_slice_in_dim(tokens, col_start, col_width, 1)
    cot_cols = lax.dynamic_slice_in_dim(out_grad, col_start, col_width, 1)
    token_buf = jnp.where(
        used[:, None], jnp.take(token_cols, token_ids, axis=0), jnp.zeros((), jnp.bfloat16)
    ).reshape(expert_count, capacity, col_width)
    cot_buf = jnp.where(
        used[:, None], jnp.take(cot_cols, token_ids, axis=0), jnp.zeros((), jnp.bfloat16)
    ).reshape(expert_count, capacity, col_width)
    weight_buf = jnp.where(
        used, jnp.take(route_weights.reshape(-1), slot_source, axis=0), 0.0
    ).reshape(expert_count, capacity)
    half_cap = capacity // 2
    received = (
        two_step_exchange(
            token_buf.reshape(ep_size, half_cap, col_width), ("ep_0", "ep_1"), (1, 0), 0, 0
        ),
        two_step_exchange(
            cot_buf.reshape(ep_size, half_cap, col_width), ("ep_0", "ep_1"), (1, 0), 0, 0
        ),
        two_step_exchange(
            weight_buf.reshape(ep_size, half_cap).astype(jnp.bfloat16),
            ("ep_0", "ep_1"),
            (1, 0),
            0,
            0,
        ).astype(jnp.float32),
    )
    parity = lax.axis_index(EP) % 2
    joined = []
    for member in received:
        partner = partner_2(for_sending(member), EP, 0).astype(member.dtype)
        first_half = jnp.where(parity == 0, member, partner)
        second_half = jnp.where(parity == 0, partner, member)
        joined.append(jnp.concatenate([first_half, second_half], axis=1))
    x_part, dy_part, g_rows = joined
    x_rows, dy_rows = side_by_side((x_part, dy_part), "tp", 2, 0)
    row_count = ep_size * capacity
    x_flat = x_rows.reshape(row_count, model_width)
    dy_flat = dy_rows.reshape(row_count, model_width)
    g_flat = g_rows.reshape(row_count, 1)
    gate_local = gate_proj[0]
    up_local = up_proj[0]
    down_local = down_proj[0]
    pre_gate = jnp.dot(x_flat, gate_local, preferred_element_type=jnp.float32)
    pre_up = jnp.dot(x_flat, up_local, preferred_element_type=jnp.float32)
    sigma = jax.nn.sigmoid(pre_gate)
    activ = pre_gate * sigma
    hidden = activ * pre_up
    d_hidden = contract_cols(dy_flat, down_local)
    gate_part = jnp.sum(hidden * d_hidden, axis=1)
    scaled = g_flat * d_hidden
    d_gate = (scaled * pre_up * sigma * (1.0 + pre_gate * (1.0 - sigma))).astype(jnp.bfloat16)
    d_up = (scaled * activ).astype(jnp.bfloat16)
    scaled_cot = (g_flat * dy_flat.astype(jnp.float32)).astype(jnp.bfloat16)
    grad_gate = contract_rows(x_flat, d_gate).astype(jnp.bfloat16)
    grad_up = contract_rows(x_flat, d_up).astype(jnp.bfloat16)
    grad_down = contract_rows(hidden.astype(jnp.bfloat16), scaled_cot).astype(jnp.bfloat16)
    partial_value = contract_cols(d_gate, gate_local) + contract_cols(d_up, up_local)
    summed = sum_at_owner(
        partial_value.reshape(ep_size, capacity, model_width).astype(jnp.bfloat16), "tp", 2
    ).astype(jnp.bfloat16)
    gate_total = over_copies(gate_part.reshape(ep_size, capacity), "tp")
    back_rows, back_gate = (
        lax.all_to_all(summed, EP, split_axis=0, concat_axis=0, tiled=True),
        lax.all_to_all(
            gate_total.astype(jnp.bfloat16), EP, split_axis=0, concat_axis=0, tiled=True
        ).astype(gate_total.dtype),
    )
    col_count = back_rows.shape[2]
    pair_rows = (
        back_rows.astype(jnp.float32)
        .reshape(expert_count, 2, capacity, col_count)
        .sum(axis=1)
        .reshape(slot_count, col_count)
    )
    pair_gate = back_gate.reshape(expert_count, 2, capacity).sum(axis=1).reshape(slot_count)
    tokens_grad = (
        jnp.take(pair_rows, destination, axis=0)
        .reshape(token_count, top_count, col_count)
        .sum(axis=1)
        .astype(jnp.bfloat16)
    )
    route_grad = jnp.take(pair_gate, destination, axis=0).reshape(token_count, top_count)
    return (tokens_grad, route_grad, grad_gate[None], grad_up[None], grad_down[None])


def solution(mesh):
    torus = Mesh(mesh.devices.reshape(16, 2, mesh.shape["tp"]), ("ep_0", "ep_1", "tp"))
    placed = (
        P(EP, None),
        P(EP, None),
        P(EP, None),
        P(EP, None),
        P(EP, None, "tp"),
        P(EP, None, "tp"),
        P(EP, "tp", None),
    )
    return jax.shard_map(
        local,
        mesh=torus,
        in_specs=placed,
        out_specs=(
            P(EP, "tp"),
            P(EP, None),
            P(EP, None, "tp"),
            P(EP, None, "tp"),
            P(EP, "tp", None),
        ),
        check_vma=False,
    )
```

profile of v0, /device:TPU:1, one launch (start us, length us, event | category | flops | bytes accessed | tf_op | source)
XLA Modules:
  0.0 273.0 jit_solution(4949737060180148677)
XLA Ops:
  7.2 0.8 copy.90
  9.4 1.4 scatter_custom_fusion.1
  10.8 0.8 constant_dynamic-slice_fusion
  11.6 1.4 gather_fusion.4
  13.0 1.4 gather_fusion.3
  14.4 1.5 scatter_custom_fusion
  16.8 10.1 %all-to-all-start.2 = ((bf16[16,2,1,9,128]{4,0,3,2,1:T(8,128)(2,1)}), bf16[16,2,1,9,128]{4,0,3,2,1:T(8,128)(2,1)S(1)}, u32[]{:S(2)}, u32[]{:S(2)}) async-start(bf16[16,2,1,9,128]{4,0,3,2,1:T(8,128)(2,1)} %copy.97), calls=%async_computation.2 | async-start | bytes 147456 | tf_op jit(solution)/shard_map/all_to_all | solution.py:25
  28.0 3.6 %all-to-all-start.4 = ((bf16[16,2,1,9,128]{4,0,3,2,1:T(8,128)(2,1)}), bf16[16,2,1,9,128]{4,0,3,2,1:T(8,128)(2,1)S(1)}, u32[]{:S(2)}, u32[]{:S(2)}) async-start(bf16[16,2,1,9,128]{4,0,3,2,1:T(8,128)(2,1)} %copy.100), calls=%async_computation.4 | async-start | bytes 147456 | tf_op jit(solution)/shard_map/all_to_all | solution.py:25
  32.7 9.6 %all-to-all-start.3 = ((bf16[16,2,1,9,128]{4,1,3,2,0:T(2,128)(2,1)}), bf16[16,2,1,9,128]{4,1,3,2,0:T(2,128)(2,1)S(1)}, u32[]{:S(2)}, u32[]{:S(2)}) async-start(bf16[16,2,1,9,128]{4,1,3,2,0:T(2,128)(2,1)} %copy.98), calls=%async_computation.3 | async-start | bytes 147456 | tf_op jit(solution)/shard_map/all_to_all | solution.py:25
  43.0 11.0 %all-to-all-done.3 = bf16[16,2,1,9,128]{4,1,3,2,0:T(2,128)(2,1)S(1)} async-done(((bf16[16,2,1,9,128]{4,1,3,2,0:T(2,128)(2,1)}), bf16[16,2,1,9,128]{4,1,3,2,0:T(2,128)(2,1)S(1)}, u32[]{:S(2)}, u32[]{:S(2)}) %all-to-all-start.3) | async-done | bytes 73760 | tf_op jit(solution)/shard_map/all_to_all | solution.py:25
  54.0 4.2 %all-to-all-start.5 = ((bf16[16,2,1,9,128]{4,1,3,2,0:T(2,128)(2,1)}), bf16[16,2,1,9,128]{4,1,3,2,0:T(2,128)(2,1)S(1)}, u32[]{:S(2)}, u32[]{:S(2)}) async-start(bf16[16,2,1,9,128]{4,1,3,2,0:T(2,128)(2,1)} %copy.101), calls=%async_computation.5 | async-start | bytes 147456 | tf_op jit(solution)/shard_map/all_to_all | solution.py:25
  58.3 3.3 %collective-permute-start.1 = (bf16[32,9,128]{2,0,1:T(8,128)(2,1)S(1)}, bf16[32,9,128]{2,0,1:T(8,128)(2,1)S(1)}, u32[]{:S(2)}, u32[]{:S(2)}) collective-permute-start(bf16[32,9,128]{2,0,1:T(8,128)(2,1)S(1)} %bitcast.78), channel_id=1, source_target_pairs={{0,16},{16,0},{32,48},{48,32},{64,80},{80,64},{96,112},{112,96},{1... | collective-permute-start | bytes 221192 | tf_op jit(solution)/shard_map/ppermute | solution.py:44
  61.6 8.3 %all-to-all-done.5 = bf16[16,2,1,9,128]{4,1,3,2,0:T(2,128)(2,1)S(1)} async-done(((bf16[16,2,1,9,128]{4,1,3,2,0:T(2,128)(2,1)}), bf16[16,2,1,9,128]{4,1,3,2,0:T(2,128)(2,1)S(1)}, u32[]{:S(2)}, u32[]{:S(2)}) %all-to-all-start.5) | async-done | bytes 73760 | tf_op jit(solution)/shard_map/all_to_all | solution.py:25
  70.0 4.2 %collective-permute-start.2 = (bf16[32,9,128]{2,0,1:T(8,128)(2,1)S(1)}, bf16[32,9,128]{2,0,1:T(8,128)(2,1)S(1)}, u32[]{:S(2)}, u32[]{:S(2)}) collective-permute-start(bf16[32,9,128]{2,0,1:T(8,128)(2,1)S(1)} %bitcast.80), channel_id=1, source_target_pairs={{0,16},{16,0},{32,48},{48,32},{64,80},{80,64},{96,112},{112,96},{1... | collective-permute-start | bytes 221192 | tf_op jit(solution)/shard_map/ppermute | solution.py:44
  74.2 0.9 collective-permute-done.2
  76.2 2.4 gather_fusion
  78.7 3.7 %all_to_all.51 = bf16[16,2,1,9]{3,0,2,1:T(8,128)(2,1)S(1)} all-to-all(bf16[16,2,1,9]{3,0,2,1:T(8,128)(2,1)S(1)} %copy.95), channel_id=1, replica_groups=mesh['ep_0'=16,'ep_1'=2,'tp'=16] {'ep_1'}, dimensions={1} | all-to-all | bytes 1152 | tf_op jit(solution)/shard_map/all_to_all | solution.py:25
  82.4 14.0 %all_to_all.52 = bf16[16,2,1,9]{3,1,2,0:T(2,128)(2,1)S(1)} all-to-all(bf16[16,2,1,9]{3,1,2,0:T(2,128)(2,1)S(1)} %copy.96), channel_id=1, replica_groups=mesh['ep_0'=16,'ep_1'=2,'tp'=16] {'ep_0'}, dimensions={0} | all-to-all | bytes 1152 | tf_op jit(solution)/shard_map/all_to_all | solution.py:25
  96.4 3.8 %collective-permute-start = (bf16[32,9]{1,0:T(8,128)(2,1)S(1)}, bf16[32,9]{1,0:T(8,128)(2,1)S(1)}, u32[]{:S(2)}, u32[]{:S(2)}) collective-permute-start(bf16[32,9]{1,0:T(8,128)(2,1)S(1)} %bitcast.83), channel_id=1, source_target_pairs={{0,16},{16,0},{32,48},{48,32},{64,80},{80,64},{96,112},{112,96},{1... | collective-permute-start | bytes 1736 | tf_op jit(solution)/shard_map/ppermute | solution.py:44
  101.1 40.3 %all-gather.2.cloned.1.call-done = bf16[64,18,2048]{2,0,1:T(8,128)(2,1)} async-done(((bf16[64,18,128]{2,0,1:T(8,128)(2,1)}), bf16[64,18,2048]{2,0,1:T(8,128)(2,1)}) %all-gather.2.cloned.1.call-update) | async-done | bytes 4718608 | tf_op jit(solution)/shard_map/all_gather | solution.py:50
  141.4 2.8 %fusion.28 = (bf16[32,18,2048]{2,0,1:T(8,128)(2,1)S(1)}, bf16[32,18,2048]{2,0,1:T(8,128)(2,1)S(1)}) fusion(bf16[64,18,2048]{2,0,1:T(8,128)(2,1)} %all-gather.2.cloned.1.call-done), kind=kLoop, calls=%fused_computation.81 | loop fusion | bytes 9437184 | tf_op jit(solution)/shard_map/split | solution.py:51
  144.2 3.1 %copy.103 = bf16[32,18,2048]{2,1,0:T(8,128)(2,1)} copy(bf16[32,18,2048]{2,0,1:T(8,128)(2,1)S(1)} %get-tuple-element.40) | data formatting | bytes 4718592 | tf_op jit(solution)/shard_map/split | solution.py:51
  147.2 4.3 %reshape.144 = bf16[576,2048]{1,0:T(8,128)(2,1)} reshape(bf16[32,18,2048]{2,1,0:T(8,128)(2,1)} %copy.103) | data formatting | bytes 4718592 | tf_op jit(solution)/shard_map/reshape | solution.py:144
  151.6 3.1 %copy.104 = bf16[32,18,2048]{2,1,0:T(8,128)(2,1)} copy(bf16[32,18,2048]{2,0,1:T(8,128)(2,1)S(1)} %get-tuple-element.41) | data formatting | bytes 4718592 | tf_op jit(solution)/shard_map/split | solution.py:51
  154.6 2.9 %reshape.145 = bf16[576,2048]{1,0:T(8,128)(2,1)S(1)} reshape(bf16[32,18,2048]{2,1,0:T(8,128)(2,1)} %copy.104) | data formatting | bytes 4718592 | tf_op jit(solution)/shard_map/reshape | solution.py:143
  157.6 0.8 fusion.7
  158.6 0.8 fusion.10
  159.4 1.0 copy-done.1
  160.5 1.5 multiply_reduce_fusion
  162.9 1.7 reshape.222
  164.6 4.7 %all-to-all-start.8 = ((f32[16,1,576]{2,1,0:T(1,128)}), f32[16,1,576]{2,1,0:T(1,128)S(1)}, u32[]{:S(2)}, u32[]{:S(2)}) async-start(f32[16,1,576]{2,1,0:T(1,128)} %reshape.222), calls=%async_computation.8 | async-start | bytes 81920 | tf_op jit(solution)/shard_map/all_to_all | solution.py:62
  169.3 1.7 fusion.5
  171.0 0.8 fusion.4
  172.5 2.4 copy.117
  174.9 0.8 all-to-all-done.8
  176.3 5.9 %all-to-all-start.6 = ((bf16[16,32,18,128]{3,1,2,0:T(8,128)(2,1)}), bf16[16,32,18,128]{3,1,2,0:T(8,128)(2,1)}, u32[]{:S(2)}, u32[]{:S(2)}) async-start(bf16[16,32,18,128]{3,1,2,0:T(8,128)(2,1)} %bitcast.75), calls=%async_computation.6 | async-start | bytes 4718592 | tf_op jit(solution)/shard_map/all_to_all | solution.py:56
  182.9 1.5 reduce.3
  185.2 25.5 %all-to-all-done.6 = bf16[16,32,18,128]{3,1,2,0:T(8,128)(2,1)} async-done(((bf16[16,32,18,128]{3,1,2,0:T(8,128)(2,1)}), bf16[16,32,18,128]{3,1,2,0:T(8,128)(2,1)}, u32[]{:S(2)}, u32[]{:S(2)}) %all-to-all-start.6) | async-done | bytes 2359328 | tf_op jit(solution)/shard_map/all_to_all | solution.py:56
  210.7 18.4 %all-to-all-start.9 = ((bf16[32,1,18]{2,1,0:T(2,128)(2,1)}), bf16[32,1,18]{2,1,0:T(2,128)(2,1)S(1)}, u32[]{:S(2)}, u32[]{:S(2)}) async-start(bf16[32,1,18]{2,1,0:T(2,128)(2,1)} %copy.110), calls=%async_computation.9 | async-start | bytes 32768 | tf_op jit(solution)/shard_map/all_to_all | solution.py:170
  229.1 1.7 fusion.1
  230.9 2.0 reduce_sum.73
  233.6 7.3 %all-to-all-done.9 = bf16[32,1,18]{2,1,0:T(2,128)(2,1)S(1)} async-done(((bf16[32,1,18]{2,1,0:T(2,128)(2,1)}), bf16[32,1,18]{2,1,0:T(2,128)(2,1)S(1)}, u32[]{:S(2)}, u32[]{:S(2)}) %all-to-all-start.9) | async-done | bytes 1184 | tf_op jit(solution)/shard_map/all_to_all | solution.py:170
  240.9 5.1 %all-to-all-start.7 = ((bf16[32,18,128]{2,1,0:T(8,128)(2,1)}), bf16[32,18,128]{2,1,0:T(8,128)(2,1)S(1)}, u32[]{:S(2)}, u32[]{:S(2)}) async-start(bf16[32,18,128]{2,1,0:T(8,128)(2,1)} %copy.106), calls=%async_computation.7 | async-start | bytes 393216 | tf_op jit(solution)/shard_map/all_to_all | solution.py:169
  246.0 2.8 %fusion.2 = bf16[1,2048,128]{2,1,0:T(8,128)(2,1)} fusion(bf16[576,2048]{1,0:T(8,128)(2,1)S(1)} %reshape.145, bf16[576,128]{1,0:T(8,128)(2,1)} %get-tuple-element.44), kind=kOutput, calls=%fused_computation.15 | convolution fusion | flops 302252032 | bytes 3031040 | tf_op jit(solution)/shard_map/dot_general | solution.py:81
  248.7 2.6 fusion.3
  251.5 1.9 gather_fusion.2
  254.2 10.3 %all-to-all-done.7 = bf16[32,18,128]{2,1,0:T(8,128)(2,1)S(1)} async-done(((bf16[32,18,128]{2,1,0:T(8,128)(2,1)}), bf16[32,18,128]{2,1,0:T(8,128)(2,1)S(1)}, u32[]{:S(2)}, u32[]{:S(2)}) %all-to-all-start.7) | async-done | bytes 147488 | tf_op jit(solution)/shard_map/all_to_all | solution.py:169
  265.3 0.9 select_reduce_fusion
  (87 shorter events, 13.8 us)
Async XLA Ops:
  7.2 150.4 %copy-start = (bf16[1,2048,128]{2,1,0:T(8,128)(2,1)S(1)}, bf16[1,2048,128]{2,1,0:T(8,128)(2,1)}, u32[]{:S(2)}) copy-start(bf16[1,2048,128]{2,1,0:T(8,128)(2,1)} %param.13) | copy-start | bytes 1572868
  13.0 62.9 %copy-start.10 = (f32[128,2]{0,1:T(2,128)S(1)}, f32[128,2]{0,1:T(2,128)}, u32[]{:S(2)}) copy-start(f32[128,2]{0,1:T(2,128)} %param.11) | copy-start | bytes 3076
  16.8 11.2 %all-to-all-start.2 = ((bf16[16,2,1,9,128]{4,0,3,2,1:T(8,128)(2,1)}), bf16[16,2,1,9,128]{4,0,3,2,1:T(8,128)(2,1)S(1)}, u32[]{:S(2)}, u32[]{:S(2)}) async-start(bf16[16,2,1,9,128]{4,0,3,2,1:T(8,128)(2,1)} %copy.97), calls=%async_computation.2 | async-start | bytes 147456 | tf_op jit(solution)/shard_map/all_to_all | solution.py:25
  28.0 4.7 %all-to-all-start.4 = ((bf16[16,2,1,9,128]{4,0,3,2,1:T(8,128)(2,1)}), bf16[16,2,1,9,128]{4,0,3,2,1:T(8,128)(2,1)S(1)}, u32[]{:S(2)}, u32[]{:S(2)}) async-start(bf16[16,2,1,9,128]{4,0,3,2,1:T(8,128)(2,1)} %copy.100), calls=%async_computation.4 | async-start | bytes 147456 | tf_op jit(solution)/shard_map/all_to_all | solution.py:25
  32.7 21.3 %all-to-all-start.3 = ((bf16[16,2,1,9,128]{4,1,3,2,0:T(2,128)(2,1)}), bf16[16,2,1,9,128]{4,1,3,2,0:T(2,128)(2,1)S(1)}, u32[]{:S(2)}, u32[]{:S(2)}) async-start(bf16[16,2,1,9,128]{4,1,3,2,0:T(2,128)(2,1)} %copy.98), calls=%async_computation.3 | async-start | bytes 147456 | tf_op jit(solution)/shard_map/all_to_all | solution.py:25
  54.0 15.9 %all-to-all-start.5 = ((bf16[16,2,1,9,128]{4,1,3,2,0:T(2,128)(2,1)}), bf16[16,2,1,9,128]{4,1,3,2,0:T(2,128)(2,1)S(1)}, u32[]{:S(2)}, u32[]{:S(2)}) async-start(bf16[16,2,1,9,128]{4,1,3,2,0:T(2,128)(2,1)} %copy.101), calls=%async_computation.5 | async-start | bytes 147456 | tf_op jit(solution)/shard_map/all_to_all | solution.py:25
  58.2 83.2 %all-gather.2.cloned.1.call-start = ((), (), s32[]{:S(2)}) async-start(), calls=%async_computation.10 | async-start | bytes 5013504 | tf_op jit(solution)/shard_map/all_gather | solution.py:50
  58.3 15.9 %collective-permute-start.1 = (bf16[32,9,128]{2,0,1:T(8,128)(2,1)S(1)}, bf16[32,9,128]{2,0,1:T(8,128)(2,1)S(1)}, u32[]{:S(2)}, u32[]{:S(2)}) collective-permute-start(bf16[32,9,128]{2,0,1:T(8,128)(2,1)S(1)} %bitcast.78), channel_id=1, source_target_pairs={{0,16},{16,0},{32,48},{48,32},{64,80},{80,64},{96,112},{112,96},{1... | collective-permute-start | bytes 221192 | tf_op jit(solution)/shard_map/ppermute | solution.py:44
  70.0 5.1 %collective-permute-start.2 = (bf16[32,9,128]{2,0,1:T(8,128)(2,1)S(1)}, bf16[32,9,128]{2,0,1:T(8,128)(2,1)S(1)}, u32[]{:S(2)}, u32[]{:S(2)}) collective-permute-start(bf16[32,9,128]{2,0,1:T(8,128)(2,1)S(1)} %bitcast.80), channel_id=1, source_target_pairs={{0,16},{16,0},{32,48},{48,32},{64,80},{80,64},{96,112},{112,96},{1... | collective-permute-start | bytes 221192 | tf_op jit(solution)/shard_map/ppermute | solution.py:44
  96.4 4.5 %collective-permute-start = (bf16[32,9]{1,0:T(8,128)(2,1)S(1)}, bf16[32,9]{1,0:T(8,128)(2,1)S(1)}, u32[]{:S(2)}, u32[]{:S(2)}) collective-permute-start(bf16[32,9]{1,0:T(8,128)(2,1)S(1)} %bitcast.83), channel_id=1, source_target_pairs={{0,16},{16,0},{32,48},{48,32},{64,80},{80,64},{96,112},{112,96},{1... | collective-permute-start | bytes 1736 | tf_op jit(solution)/shard_map/ppermute | solution.py:44
  157.6 1.0 copy-start.3
  158.6 0.8 copy-start.4
  158.6 1.8 copy-start.1
  158.6 1.9 copy-start.11
  160.5 1.5 copy-start.6
  164.6 11.1 %all-to-all-start.8 = ((f32[16,1,576]{2,1,0:T(1,128)}), f32[16,1,576]{2,1,0:T(1,128)S(1)}, u32[]{:S(2)}, u32[]{:S(2)}) async-start(f32[16,1,576]{2,1,0:T(1,128)} %reshape.222), calls=%async_computation.8 | async-start | bytes 81920 | tf_op jit(solution)/shard_map/all_to_all | solution.py:62
  169.2 1.7 copy-start.7
  175.7 0.6 copy-start.9
  175.7 53.4 %copy-start.8 = (bf16[576,128]{1,0:T(8,128)(2,1)S(1)}, bf16[576,128]{1,0:T(8,128)(2,1)}, u32[]{:S(2)}) copy-start(bf16[576,128]{1,0:T(8,128)(2,1)} %get-tuple-element.43) | copy-start | bytes 442372
  176.3 34.4 %all-to-all-start.6 = ((bf16[16,32,18,128]{3,1,2,0:T(8,128)(2,1)}), bf16[16,32,18,128]{3,1,2,0:T(8,128)(2,1)}, u32[]{:S(2)}, u32[]{:S(2)}) async-start(bf16[16,32,18,128]{3,1,2,0:T(8,128)(2,1)} %bitcast.75), calls=%async_computation.6 | async-start | bytes 4718592 | tf_op jit(solution)/shard_map/all_to_all | solution.py:56
  210.7 30.2 %all-to-all-start.9 = ((bf16[32,1,18]{2,1,0:T(2,128)(2,1)}), bf16[32,1,18]{2,1,0:T(2,128)(2,1)S(1)}, u32[]{:S(2)}, u32[]{:S(2)}) async-start(bf16[32,1,18]{2,1,0:T(2,128)(2,1)} %copy.110), calls=%async_computation.9 | async-start | bytes 32768 | tf_op jit(solution)/shard_map/all_to_all | solution.py:170
  233.6 15.1 %copy-start.5 = (f32[576,128]{1,0:T(8,128)S(1)}, f32[576,128]{1,0:T(8,128)}, u32[]{:S(2)}) copy-start(f32[576,128]{1,0:T(8,128)} %copy-done.4) | copy-start | bytes 884740
  240.9 23.6 %all-to-all-start.7 = ((bf16[32,18,128]{2,1,0:T(8,128)(2,1)}), bf16[32,18,128]{2,1,0:T(8,128)(2,1)S(1)}, u32[]{:S(2)}, u32[]{:S(2)}) async-start(bf16[32,18,128]{2,1,0:T(8,128)(2,1)} %copy.106), calls=%async_computation.7 | async-start | bytes 393216 | tf_op jit(solution)/shard_map/all_to_all | solution.py:169
  245.9 2.8 %copy-start.2 = (bf16[576,2048]{1,0:T(8,128)(2,1)S(1)}, bf16[576,2048]{1,0:T(8,128)(2,1)}, u32[]{:S(2)}) copy-start(bf16[576,2048]{1,0:T(8,128)(2,1)} %reshape.144) | copy-start | bytes 7077892
Sparse Core Ops, SparseCore 0:
  76.0 65.3 all-gather.1
where the time goes:
time: 274 us; the launch traced here: 273 us
  waiting for transfers between devices  106 us (39%)
  starting transfers between devices  72.8 us (27%)
  local copies, waits for them, and re-layouts  43.2 us (16%)
  blocking collectives  17.7 us (6%)
  between operations  14.5 us (5%)
  matrix products  12.6 us (5%)
  other arithmetic  6.32 us (2%)
    all_gather x1, waiting for transfers between devices, side_by_side(): result = lax.all_gather(both, axis, axis=dim, tiled=True)  40.3 us
    all_to_all x4, starting transfers between devices, moved_by_axis(): result = lax.all_to_all(result, axes[k], k, k, tiled=True)  27.5 us
    all_to_all x1, waiting for transfers between devices, sum_at_owner(): lax.all_to_all(cut_along(array, dim, length), axis, 0, 0, tiled=True)  25.5 us
    all_to_all x4, waiting for transfers between devices, moved_by_axis(): result = lax.all_to_all(result, axes[k], k, k, tiled=True)  20.1 us
    all_to_all x1, starting transfers between devices, local(): lax.all_to_all(gate_total.astype(jnp.bfloat16), EP, split_axis=0, concat_...  18.4 us
    all_to_all x2, blocking collectives, moved_by_axis(): result = lax.all_to_all(result, axes[k], k, k, tiled=True)  17.7 us
    ppermute x3, starting transfers between devices, partner_2(): lax.ppermute(array, axis, [(i, i ^ 1 << apart) for i in range(lax.axis_si...  11.3 us
    all_to_all x1, waiting for transfers between devices, local(): lax.all_to_all(summed, EP, split_axis=0, concat_axis=0, tiled=True)  10.3 us
  transfers between devices with their start and end apart: 12, of which 11 were waited for; matrix products, arithmetic and copies ran while one was open for 10% of the time, Pallas kernels for 0%

commit v1 on v0

v1 whole, which is shorter than its diff:
```python
import jax
import jax.numpy as jnp
from jax import lax
from jax.experimental import pallas as pl
from jax.experimental.pallas import tpu as pltpu
from jax.sharding import PartitionSpec as P

MESH = pl.DeviceIdType.MESH
F32, BF16 = jnp.float32, jnp.bfloat16
NZ, SIDE = 16, 4
CAP, PAD = 18, 32
LANES = 128
MODEL = 2048
HALF_ROWS = NZ * CAP
ROWS = 2 * HALF_ROWS
QUARTER = HALF_ROWS // 2
HIGHEST = lax.Precision.HIGHEST


def dot(left, right, dims, precision=None):
    return lax.dot_general(
        left, right, ((dims[:1], dims[1:]), ((), ())), precision=precision,
        preferred_element_type=F32,
    )


def far_first(i):
    step = (i + 1) // 2
    return NZ // 2 + step * (1 - 2 * (i % 2))


def kernel(
    routes, weights, tok_hbm, cot_hbm, gate_hbm, up_hbm, down_hbm,
    out_tok, out_route, out_gate, out_up, out_down,
    tok_v, cot_v, wgu, down_v, pall, send, recv, pad, xs, dgu, hid, prod,
    dother, crecv, dacc, rs, r1, r2, send2, q1, q2, fin, ret, home,
    g0, g1, g2, ga, gb, gc, gs, gr, og, ou, od,
    in_sem, out_sem, z_send, z_recv, s1, n1, s2, n2, ps, pn,
    cs, cn, rs_send, rs_recv, qs, qn, fs, fn, gas, gan, gbs, gbn, gcs, gcn, gzs, gzn,
):
    ep, t = lax.axis_index("ep"), lax.axis_index("tp")
    z, c = ep // 2, ep % 2
    y, x = t // SIDE, t % SIDE
    p1, p2 = x + c * (y - x), y + c * (x - y)
    w1, w2 = 1 + 3 * c, 4 - 3 * c

    def block(o1, o2):
        return w1 * ((p1 + o1) % SIDE) + w2 * ((p2 + o2) % SIDE)

    def block_of_partner(o1, o2):
        return w2 * ((p2 + o1) % SIDE) + w1 * ((p1 + o2) % SIDE)

    def along1(o):
        return (ep, block(o, 0))

    def along2(o):
        return (ep, block(0, o))

    partner = (z * 2 + 1 - c, t)

    def remote(src, dst, send_sem, recv_sem, device):
        return pltpu.make_async_remote_copy(
            src_ref=src, dst_ref=dst, send_sem=send_sem, recv_sem=recv_sem,
            device_id=device, device_id_type=MESH,
        )

    barrier = pltpu.get_barrier_semaphore()

    def greet(i, carry):
        pl.semaphore_signal(barrier, inc=1, device_id=((ep + i) % (2 * NZ), t), device_id_type=MESH)
        return carry

    lax.fori_loop(1, 2 * NZ, greet, 0)
    for o in range(1, SIDE):
        pl.semaphore_signal(barrier, inc=1, device_id=along1(o), device_id_type=MESH)
        pl.semaphore_signal(barrier, inc=1, device_id=along2(o), device_id_type=MESH)

    own_cols = pl.ds(pl.multiple_of(t * LANES, LANES), LANES)
    loads = [
        pltpu.make_async_copy(tok_hbm.at[:, own_cols], tok_v, in_sem.at[0]),
        pltpu.make_async_copy(cot_hbm.at[:, own_cols], cot_v, in_sem.at[1]),
        pltpu.make_async_copy(gate_hbm.at[0], wgu.at[:, pl.ds(0, LANES)], in_sem.at[2]),
        pltpu.make_async_copy(up_hbm.at[0], wgu.at[:, pl.ds(LANES, LANES)], in_sem.at[3]),
        pltpu.make_async_copy(down_hbm.at[0], down_v, in_sem.at[4]),
    ]
    for load in loads:
        load.start()

    r0, r1_ = routes[0:1, :], routes[1:2, :]
    experts = lax.broadcasted_iota(jnp.int32, (NZ, LANES), 0)
    hit0, hit1 = experts == r0, experts == r1_
    named = jnp.logical_or(hit0, hit1)
    earlier_than = (
        lax.broadcasted_iota(jnp.int32, (LANES, LANES), 0)
        < lax.broadcasted_iota(jnp.int32, (LANES, LANES), 1)
    ).astype(BF16)
    earlier = dot(named.astype(F32).astype(BF16), earlier_than, (1, 0))
    place = jnp.where(named, earlier, -1.0)
    weight = jnp.where(hit0, weights[0:1, :], 0.0) + jnp.where(hit1, weights[1:2, :], 0.0)
    slot_ids = lax.broadcasted_iota(jnp.int32, (PAD, LANES), 0).astype(F32)
    gains = []
    for e in range(NZ):
        picked = slot_ids == place[e : e + 1, :]
        pall[PAD * e : PAD * (e + 1), :] = picked.astype(F32).astype(BF16)
        gains.append(
            jnp.sum(jnp.where(picked, weight[e : e + 1, :], 0.0), axis=1, keepdims=True)
        )
    pad[...] = jnp.zeros_like(pad)
    home[...] = jnp.zeros_like(home)
    loads[0].wait()
    rows = dot(pall[...], tok_v[...], (1, 0)).astype(BF16)
    for e in range(NZ):
        send[0, e] = rows[PAD * e : PAD * e + CAP, :]
    loads[1].wait()
    rows = dot(pall[...], cot_v[...], (1, 0))
    for e in range(NZ):
        send[1, e] = (rows[PAD * e : PAD * e + CAP, :] * gains[e][:CAP, :]).astype(BF16)
    squeeze_r = lax.broadcasted_iota(jnp.int32, (QUARTER, 8 * PAD), 0)
    squeeze_p = lax.broadcasted_iota(jnp.int32, (QUARTER, 8 * PAD), 1)
    slot = squeeze_p % PAD
    squeeze = jnp.logical_and(
        squeeze_r == (squeeze_p // PAD) * CAP + slot, slot < CAP
    ).astype(F32)
    squeeze_b = squeeze.astype(BF16)

    pl.semaphore_wait(barrier, 2 * NZ - 1 + 2 * (SIDE - 1))

    def to_same(dz):
        i = c * NZ + dz
        to = (z + dz) % NZ
        return remote(send.at[c, to], recv.at[i], z_send.at[0, dz], z_recv.at[i], (to * 2 + c, t))

    def to_other(dz):
        i = c * NZ + dz
        to = (z + dz) % NZ
        return remote(
            send.at[1 - c, to], recv.at[i], z_send.at[1, dz], z_recv.at[i], (to * 2 + 1 - c, t)
        )

    def dispatch(i, carry):
        dz = far_first(i)
        to_same(dz).start()
        to_other(dz).start()
        return carry

    lax.fori_loop(0, NZ - 1, dispatch, 0)
    to_other(0).start()
    recv[c * NZ] = send[c, z]

    def arrived(i):
        remote(recv.at[i], recv.at[i], z_send.at[0, 0], z_recv.at[i], partner).wait_recv()

    arrived((1 - c) * NZ)

    def arrive(dz, carry):
        arrived(dz)
        arrived(NZ + dz)
        return carry

    lax.fori_loop(1, NZ, arrive, 0)
    for i in range(2 * NZ):
        pad[PAD * i : PAD * i + CAP, :] = recv[i]
    for k in range(4):
        xs[c, QUARTER * k : QUARTER * (k + 1), own_cols] = dot(
            squeeze_b, pad[8 * PAD * k : 8 * PAD * (k + 1), :], (1, 0)
        ).astype(BF16)

    waits = []

    def piece(o1, o2, first, count):
        cols = pl.ds(pl.multiple_of(block(o1, o2) * LANES, LANES), LANES)
        return xs.at[c, pl.ds(first, count), cols]

    WHOLE, LOW, HIGH = (0, ROWS), (0, HALF_ROWS), (HALF_ROWS, HALF_ROWS)

    def pass_on(o1, o2, part, send_sem, recv_sem, device):
        ref = piece(o1, o2, *part)
        copy = remote(ref, ref, send_sem, recv_sem, device)
        copy.start()
        waits.append(copy)

    def came(o1, o2, part, recv_sem):
        ref = piece(o1, o2, *part)
        remote(ref, ref, recv_sem, recv_sem, partner).wait_recv()

    def hand_over(o1, o2):
        i = (o1 % SIDE) * SIDE + o2 % SIDE
        pass_on(o1, o2, WHOLE, ps.at[i], pn.at[i], partner)

    def both_ways(o1):
        j = o1 % SIDE
        pass_on(o1, 0, WHOLE, s2.at[j, 0], n2.at[j, 0], along2(1))
        pass_on(o1, 0, WHOLE, s2.at[j, 1], n2.at[j, 1], along2(-1))

    pass_on(0, 0, WHOLE, s1.at[0], n1.at[0], along1(1))
    pass_on(0, 0, WHOLE, s1.at[1], n1.at[1], along1(-1))
    both_ways(0)
    hand_over(0, 0)
    came(-1, 0, WHOLE, n1.at[0])
    pass_on(-1, 0, LOW, s1.at[2], n1.at[2], along1(1))
    both_ways(-1)
    hand_over(-1, 0)
    came(1, 0, WHOLE, n1.at[1])
    pass_on(1, 0, HIGH, s1.at[3], n1.at[3], along1(-1))
    both_ways(1)
    hand_over(1, 0)

    def across(o1):
        j = o1 % SIDE
        came(o1, -1, WHOLE, n2.at[j, 0])
        pass_on(o1, -1, LOW, s2.at[j, 2], n2.at[j, 2], along2(1))
        hand_over(o1, -1)
        came(o1, 1, WHOLE, n2.at[j, 1])
        pass_on(o1, 1, HIGH, s2.at[j, 3], n2.at[j, 3], along2(-1))
        hand_over(o1, 1)

    across(0)
    came(2, 0, LOW, n1.at[2])
    came(2, 0, HIGH, n1.at[3])
    both_ways(2)
    hand_over(2, 0)
    for o1 in (-1, 1, 2):
        across(o1)
    for o1 in (0, -1, 1, 2):
        j = o1 % SIDE
        came(o1, 2, LOW, n2.at[j, 2])
        came(o1, 2, HIGH, n2.at[j, 3])
        hand_over(o1, 2)
    for o1 in range(SIDE):
        for o2 in range(SIDE):
            cols = pl.ds(pl.multiple_of(block_of_partner(o1, o2) * LANES, LANES), LANES)
            ref = xs.at[1 - c, :, cols]
            remote(ref, ref, pn.at[o1 * SIDE + o2], pn.at[o1 * SIDE + o2], partner).wait_recv()

    for load in loads[2:]:
        load.wait()
    pre = dot(xs[0], wgu[...], (1, 0))
    dh = dot(xs[1], down_v[...], (1, 1))
    a, b = pre[:, :LANES], pre[:, LANES:]
    sigma = jax.nn.sigmoid(a)
    activ = a * sigma
    hidden = activ * b
    dgu[:, :LANES] = (dh * b * sigma * (1.0 + a * (1.0 - sigma))).astype(BF16)
    dgu[:, LANES:] = (dh * activ).astype(BF16)
    hid[...] = hidden.astype(BF16)
    prod[...] = hidden * dh

    others = pl.ds(pl.multiple_of((1 - c) * HALF_ROWS, HALF_ROWS), HALF_ROWS)
    owns = pl.ds(pl.multiple_of(c * HALF_ROWS, HALF_ROWS), HALF_ROWS)
    order = (2, 1, 3, 0)
    combine = {}
    for o1 in order:
        for o2 in range(SIDE):
            wrows = pl.ds(pl.multiple_of(block_of_partner(o1, o2) * LANES, LANES), LANES)
            dother[o1, o2] = dot(dgu[others, :], wgu[wrows, :], (1, 1)).astype(BF16)
        combine[o1] = remote(dother.at[o1], crecv.at[o1], cs.at[o1], cn.at[o1], partner)
        combine[o1].start()
    waits.extend(combine.values())
    for o1 in order:
        for o2 in range(SIDE):
            wrows = pl.ds(pl.multiple_of(block(o1, o2) * LANES, LANES), LANES)
            dacc[o1, o2] = dot(dgu[owns, :], wgu[wrows, :], (1, 1))

    lo, hi = pl.ds(0, QUARTER), pl.ds(QUARTER, QUARTER)

    def ship(src, dst, send_sem, recv_sem, device):
        copy = remote(src, dst, send_sem, recv_sem, device)
        copy.start()
        waits.append(copy)
        return copy

    combine[2].wait_recv()
    rs[2] = (dacc[2] + crecv[2].astype(F32)).astype(BF16)
    first_up = ship(rs.at[2, :, lo], r1.at[0], rs_send.at[0], rs_recv.at[0], along1(1))
    first_down = ship(rs.at[2, :, hi], r1.at[1], rs_send.at[1], rs_recv.at[1], along1(-1))
    combine[1].wait_recv()
    rs[1, :, hi] = (dacc[1, :, hi] + crecv[1, :, hi].astype(F32)).astype(BF16)
    up_hi = ship(rs.at[1, :, hi], r2.at[0, :, hi], rs_send.at[2], rs_recv.at[2], along1(1))
    combine[3].wait_recv()
    rs[3, :, lo] = (dacc[3, :, lo] + crecv[3, :, lo].astype(F32)).astype(BF16)
    down_lo = ship(rs.at[3, :, lo], r2.at[1, :, lo], rs_send.at[3], rs_recv.at[3], along1(-1))
    first_up.wait_recv()
    rs[1, :, lo] = (
        dacc[1, :, lo] + crecv[1, :, lo].astype(F32) + r1[0].astype(F32)
    ).astype(BF16)
    up_lo = ship(rs.at[1, :, lo], r2.at[0, :, lo], rs_send.at[4], rs_recv.at[4], along1(1))
    first_down.wait_recv()
    rs[3, :, hi] = (
        dacc[3, :, hi] + crecv[3, :, hi].astype(F32) + r1[1].astype(F32)
    ).astype(BF16)
    down_hi = ship(rs.at[3, :, hi], r2.at[1, :, hi], rs_send.at[5], rs_recv.at[5], along1(-1))

    for k in range(4):
        spread = dot(squeeze, prod[QUARTER * k : QUARTER * (k + 1), :], (0, 0), HIGHEST)
        g0[:, 8 * PAD * k : 8 * PAD * (k + 1)] = dot(
            jnp.ones((8, LANES), F32), spread, (1, 1), HIGHEST
        )
    first = [ship(g0, ga.at[o - 1], gas.at[o - 1], gan.at[o - 1], along1(o)) for o in (1, 2, 3)]

    def grads(k, carry):
        cols = pl.ds(pl.multiple_of(k * 256, 256), 256)
        part = dot(xs[0, :, cols], dgu[...], (0, 0))
        og[cols, :] = part[:, :LANES].astype(BF16)
        ou[cols, :] = part[:, LANES:].astype(BF16)
        return carry

    lax.fori_loop(0, MODEL // 256, grads, 0)
    stores = [
        pltpu.make_async_copy(og, out_gate.at[0], out_sem.at[0]),
        pltpu.make_async_copy(ou, out_up.at[0], out_sem.at[1]),
        pltpu.make_async_copy(od, out_down.at[0], out_sem.at[2]),
    ]
    stores[0].start()
    stores[1].start()
    for copy in first:
        copy.wait_recv()
    g1[...] = g0[...] + ga[0] + ga[1] + ga[2]
    second = [ship(g1, gb.at[o - 1], gbs.at[o - 1], gbn.at[o - 1], along2(o)) for o in (1, 2, 3)]

    combine[0].wait_recv()
    for copy in (up_hi, down_lo, up_lo, down_hi):
        copy.wait_recv()
    for o2 in (2, 1, 3, 0):
        dacc[0, o2] = (
            dacc[0, o2] + crecv[0, o2].astype(F32) + r2[0, o2].astype(F32) + r2[1, o2].astype(F32)
        )
        if o2:
            send2[o2] = dacc[0, o2].astype(BF16)
        if o2 == 2:
            first_up = ship(send2.at[2, lo], q1.at[0], qs.at[0], qn.at[0], along2(1))
            first_down = ship(send2.at[2, hi], q1.at[1], qs.at[1], qn.at[1], along2(-1))
        if o2 == 1:
            up_hi = ship(send2.at[1, hi], q2.at[0, hi], qs.at[2], qn.at[2], along2(1))
        if o2 == 3:
            down_lo = ship(send2.at[3, lo], q2.at[1, lo], qs.at[3], qn.at[3], along2(-1))
    for copy in second:
        copy.wait_recv()
    g2[...] = g1[...] + gb[0] + gb[1] + gb[2]
    third = ship(g2, gc, gcs.at[0], gcn.at[0], partner)
    first_up.wait_recv()
    send2[0, lo] = (dacc[0, 1, lo] + q1[0].astype(F32)).astype(BF16)
    up_lo = ship(send2.at[0, lo], q2.at[0, lo], qs.at[4], qn.at[4], along2(1))
    first_down.wait_recv()
    send2[0, hi] = (dacc[0, 3, hi] + q1[1].astype(F32)).astype(BF16)
    down_hi = ship(send2.at[0, hi], q2.at[1, hi], qs.at[5], qn.at[5], along2(-1))
    third.wait_recv()
    lanes = pl.ds(pl.multiple_of(c * NZ * PAD, NZ * PAD), NZ * PAD)
    spread = dot(
        g2[:, lanes] + gc[:, lanes], jnp.full((8, LANES), 0.125, F32), (0, 0), HIGHEST
    )
    for i in range(NZ):
        gs[i] = spread[PAD * i : PAD * i + CAP, :]

    def gate_home(dz):
        return remote(gs.at[dz], gr.at[dz], gzs.at[dz], gzn.at[dz], ((z - dz) % NZ * 2 + c, t))

    def send_gate(i, carry):
        gate_home(far_first(i)).start()
        return carry

    lax.fori_loop(0, NZ - 1, send_gate, 0)
    gr[0] = gs[0]
    for copy in (up_hi, down_lo, up_lo, down_hi):
        copy.wait_recv()
    total = (dacc[0, 0] + q2[0].astype(F32) + q2[1].astype(F32)).astype(BF16)
    for k in range(2):
        spread = dot(squeeze_b, total[QUARTER * k : QUARTER * (k + 1), :], (0, 0)).astype(BF16)
        for i in range(8):
            fin[8 * k + i] = spread[PAD * i : PAD * i + CAP, :]

    def rows_home(dz):
        return remote(fin.at[dz], ret.at[dz], fs.at[dz], fn.at[dz], ((z - dz) % NZ * 2 + c, t))

    def send_rows(i, carry):
        rows_home(far_first(i)).start()
        return carry

    lax.fori_loop(0, NZ - 1, send_rows, 0)
    ret[0] = fin[0]
    od[...] = dot(hid[...], xs[1], (0, 0)).astype(BF16)
    stores[2].start()

    def gates_came(dz, carry):
        gate_home(dz).wait_recv()
        return carry

    lax.fori_loop(1, NZ, gates_came, 0)

    def add_gates(dz, carry):
        e = (z + dz) % NZ
        at = pl.ds(pl.multiple_of(e * PAD, PAD), PAD)
        v = jnp.sum(gr[dz] * pall[at, :][:CAP, :].astype(F32), axis=0, keepdims=True)
        return (carry[0] + jnp.where(r0 == e, v, 0.0), carry[1] + jnp.where(r1_ == e, v, 0.0))

    zero = jnp.zeros((1, LANES), F32)
    v0, v1 = lax.fori_loop(0, NZ, add_gates, (zero, zero))
    out_route[0:1, :] = v0 / weights[0:1, :]
    out_route[1:2, :] = v1 / weights[1:2, :]

    def rows_came(dz, carry):
        rows_home(dz).wait_recv()
        return carry

    lax.fori_loop(1, NZ, rows_came, 0)

    def put_home(dz, carry):
        e = (z + dz) % NZ
        home[e, :CAP, :] = ret[dz]
        return carry

    lax.fori_loop(0, NZ, put_home, 0)
    out_tok[...] = dot(pall[...], home[...].reshape(NZ * PAD, LANES), (0, 0)).astype(BF16)

    def drain(dz, carry):
        to_same(dz).wait_send()
        to_other(dz).wait_send()
        gate_home(dz).wait_send()
        rows_home(dz).wait_send()
        return carry

    lax.fori_loop(1, NZ, drain, 0)
    to_other(0).wait_send()
    for copy in waits:
        copy.wait_send()
    for store in stores:
        store.wait()


def local(tokens, routes, route_weights, out_grad, gate_proj, up_proj, down_proj):
    vmem, hbm = pl.BlockSpec(memory_space=pltpu.VMEM), pl.BlockSpec(memory_space=pl.ANY)
    dma, buf = pltpu.SemaphoreType.DMA, pltpu.VMEM
    quad = (SIDE, HALF_ROWS, LANES)
    out = pl.pallas_call(
        kernel,
        out_shape=(
            jax.ShapeDtypeStruct((LANES, LANES), BF16),
            jax.ShapeDtypeStruct((2, LANES), F32),
            jax.ShapeDtypeStruct((1, MODEL, LANES), BF16),
            jax.ShapeDtypeStruct((1, MODEL, LANES), BF16),
            jax.ShapeDtypeStruct((1, LANES, MODEL), BF16),
        ),
        in_specs=[vmem, vmem, hbm, hbm, hbm, hbm, hbm],
        out_specs=[vmem, vmem, hbm, hbm, hbm],
        scratch_shapes=[
            buf((LANES, LANES), BF16),
            buf((LANES, LANES), BF16),
            buf((MODEL, 2 * LANES), BF16),
            buf((LANES, MODEL), BF16),
            buf((NZ * PAD, LANES), BF16),
            buf((2, NZ, CAP, LANES), BF16),
            buf((2 * NZ, CAP, LANES), BF16),
            buf((2 * NZ * PAD, LANES), BF16),
            buf((2, ROWS, MODEL), BF16),
            buf((ROWS, 2 * LANES), BF16),
            buf((ROWS, LANES), BF16),
            buf((ROWS, LANES), F32),
            buf((SIDE, *quad), BF16),
            buf((SIDE, *quad), BF16),
            buf((SIDE, *quad), F32),
            buf((SIDE, *quad), BF16),
            buf((2, SIDE, QUARTER, LANES), BF16),
            buf((2, *quad), BF16),
            buf(quad, BF16),
            buf((2, QUARTER, LANES), BF16),
            buf((2, HALF_ROWS, LANES), BF16),
            buf((NZ, CAP, LANES), BF16),
            buf((NZ, CAP, LANES), BF16),
            buf((NZ, PAD, LANES), BF16),
            buf((8, 2 * NZ * PAD), F32),
            buf((8, 2 * NZ * PAD), F32),
            buf((8, 2 * NZ * PAD), F32),
            buf((3, 8, 2 * NZ * PAD), F32),
            buf((3, 8, 2 * NZ * PAD), F32),
            buf((8, 2 * NZ * PAD), F32),
            buf((NZ, CAP, LANES), F32),
            buf((NZ, CAP, LANES), F32),
            buf((MODEL, LANES), BF16),
            buf((MODEL, LANES), BF16),
            buf((LANES, MODEL), BF16),
            dma((5,)),
            dma((3,)),
            dma((2, NZ)),
            dma((2 * NZ,)),
            dma((4,)),
            dma((4,)),
            dma((SIDE, 4)),
            dma((SIDE, 4)),
            dma((SIDE * SIDE,)),
            dma((SIDE * SIDE,)),
            dma((SIDE,)),
            dma((SIDE,)),
            dma((6,)),
            dma((6,)),
            dma((6,)),
            dma((6,)),
            dma((NZ,)),
            dma((NZ,)),
            dma((3,)),
            dma((3,)),
            dma((3,)),
            dma((3,)),
            dma((1,)),
            dma((1,)),
            dma((NZ,)),
            dma((NZ,)),
        ],
        compiler_params=pltpu.CompilerParams(
            collective_id=0, has_side_effects=True, vmem_limit_bytes=56 * 2**20
        ),
        name="routed_backward",
    )(routes.T, route_weights.T, tokens, out_grad, gate_proj, up_proj, down_proj)
    return (out[0], out[1].T, out[2], out[3], out[4])


def solution(mesh):
    placed = (
        P("ep", None),
        P("ep", None),
        P("ep", None),
        P("ep", None),
        P("ep", None, "tp"),
        P("ep", None, "tp"),
        P("ep", "tp", None),
    )
    return jax.shard_map(
        local,
        mesh=mesh,
        in_specs=placed,
        out_specs=(
            P("ep", "tp"),
            P("ep", None),
            P("ep", None, "tp"),
            P("ep", None, "tp"),
            P("ep", "tp", None),
        ),
        check_vma=False,
    )
```

time: 274 us -> 93.8 us (0.34)
  waiting for transfers between devices: 106 us -> 0 us
  Pallas kernels: 0 us -> 86.9 us
  starting transfers between devices: 72.8 us -> 0 us
  local copies, waits for them, and re-layouts: 43.2 us -> 5.89 us
  blocking collectives: 17.7 us -> 0 us
  between operations: 14.5 us -> 0.65 us
  matrix products: 12.6 us -> 0 us
  other arithmetic: 6.32 us -> 0 us
    pallas_call x0 -> x1, Pallas kernels: none -> 86.9 us  [local(): pl.pallas_call(kernel, out_shape=(jax.ShapeDtypeStruct((LANES, LANES), BF...]
    all_to_all x8 -> x0, waiting for transfers between devices: 64 us -> none  [the longest x1 25.5 us: sum_at_owner(): lax.all_to_all(cut_along(array, dim, length), axis, 0, 0, tiled=True)]
    all_to_all x8 -> x0, starting transfers between devices: 61.5 us -> none  [the longest x4 27.5 us: moved_by_axis(): result = lax.all_to_all(result, axes[k], k, k, tiled=True)]
    all_gather x1 -> x0, waiting for transfers between devices: 40.3 us -> none  [side_by_side(): result = lax.all_gather(both, axis, axis=dim, tiled=True)]
    all_to_all x2 -> x0, blocking collectives: 17.7 us -> none  [moved_by_axis(): result = lax.all_to_all(result, axes[k], k, k, tiled=True)]
    dot_general x8 -> x0, matrix products: 12.6 us -> none  [the longest x3 7.07 us: contract_rows(): lax.dot_general(left, right, (((0,), (0,)), ((), ())), preferred_element_...]
    ppermute x3 -> x0, starting transfers between devices: 11.3 us -> none  [partner_2(): lax.ppermute(array, axis, [(i, i ^ 1 << apart) for i in range(lax.axis_si...]
    split x3 -> x0, local copies, waits for them, and re-layouts: 8.89 us -> none  [side_by_side(): jnp.split(result, [sum(widths[:k]) for k in range(1, len(widths))], axis=...]
  transfers between devices with their start and end apart: 12 -> 0, of which waited for: 11 -> 0; matrix products, arithmetic and copies ran while one was open for 10% -> 0% of each run, Pallas kernels for 0% -> 0%
where the time goes in v1:
time: 93.8 us; the launch traced here: 93.5 us
  Pallas kernels  86.9 us (93%)
  local copies, waits for them, and re-layouts  5.89 us (6%)
    pallas_call x1, Pallas kernels, local(): pl.pallas_call(kernel, out_shape=(jax.ShapeDtypeStruct((LANES, LANES), BF...  86.9 us
    unnamed x11, local copies, waits for them, and re-layouts  5.89 us

profile of v1, /device:TPU:1, one launch (start us, length us, event | category | flops | bytes accessed | tf_op | source)
XLA Modules:
  0.0 93.5 jit_solution(10313682437511523422)
XLA Ops:
  0.6 86.9 %routed_backward.1 = (bf16[128,128]{1,0:T(8,128)(2,1)}, f32[2,128]{1,0:T(2,128)}, bf16[1,2048,128]{2,1,0:T(8,128)(2,1)}, bf16[1,2048,128]{2,1,0:T(8,128)(2,1)}, bf16[1,128,2048]{2,1,0:T(8,128)(2,1)}) custom-call(s32[2,128]{1,0:T(2,128)} %bitcast.3, f32[2,128]{1,0:T(2,128)} %bitcast.4, bf16[128,2048]{1,0:T(8,128)(2,1)} %tok_hbm.1, bf16[128,2048]{1,0:T(8,128)(2,1)} %cot_hbm.1, ...), custom_call_target="tpu_custom_call" | custom-call | tf_op jit(solution)/shard_map/routed_backward/pallas_call | solution.py:433
  87.5 0.0 copy-start.2
  87.6 1.4 %copy.17 = bf16[128,128]{1,0:T(8,128)(2,1)} copy(bf16[128,128]{1,0:T(8,128)(2,1)} %get-tuple-element.20) | data formatting | bytes 65536
  88.9 0.0 copy-done.2
  88.9 0.6 copy.18
  89.5 0.0 copy-start.1
  89.5 1.9 %copy.19 = bf16[1,2048,128]{2,1,0:T(8,128)(2,1)} copy(bf16[1,2048,128]{2,1,0:T(8,128)(2,1)} %get-tuple-element.22) | data formatting | bytes 1048576
  91.4 0.0 copy-done.1
  91.4 0.0 copy-start
  91.4 0.8 copy.20
  92.2 0.4 copy-done
  92.7 0.8 copy.21
Async XLA Ops:
  87.5 1.4 %copy-start.2 = (f32[2,128]{1,0:T(2,128)S(1)}, f32[2,128]{1,0:T(2,128)}, u32[]{:S(2)}) copy-start(f32[2,128]{1,0:T(2,128)} %get-tuple-element.11) | copy-start | bytes 3076
  89.5 1.9 %copy-start.1 = (bf16[1,2048,128]{2,1,0:T(8,128)(2,1)S(1)}, bf16[1,2048,128]{2,1,0:T(8,128)(2,1)}, u32[]{:S(2)}) copy-start(bf16[1,2048,128]{2,1,0:T(8,128)(2,1)} %get-tuple-element.23) | copy-start | bytes 1572868
  91.4 1.2 %copy-start = (bf16[1,128,2048]{2,1,0:T(8,128)(2,1)S(1)}, bf16[1,128,2048]{2,1,0:T(8,128)(2,1)}, u32[]{:S(2)}) copy-start(bf16[1,128,2048]{2,1,0:T(8,128)(2,1)} %get-tuple-element.24) | copy-start | bytes 1572868

commit v2 on v0

v2 whole, which is shorter than its diff:
```python
import jax
import jax.numpy as jnp
from jax import lax
from jax.experimental import pallas as pl
from jax.experimental.pallas import tpu as pltpu
from jax.sharding import PartitionSpec as P

MESH = pl.DeviceIdType.MESH
F32, BF16 = jnp.float32, jnp.bfloat16
NZ, SIDE = 16, 4
CAP, PAD, BACK = 18, 32, 20
LANES = 128
MODEL = 2048
ROWS = 2 * NZ * CAP
CHUNKS = 1
NEAR = NZ // CHUNKS
HALF = NEAR * CAP
PART = 2 * HALF
CUT = (HALF // 2 + 7) // 8 * 8
SELF, OTHERS = NZ - 1, (0, NZ - 1)
GATES = NEAR * PAD // LANES


def dot(left, right, dims):
    return lax.dot_general(
        left, right, ((dims[:1], dims[1:]), ((), ())), preferred_element_type=F32
    )


def away(i):
    step = NZ // 2 - (i + 1) // 2
    return step * (2 * (i % 2) - 1)


def kernel(
    routes, weights, tok_hbm, cot_hbm, gate_hbm, up_hbm, down_hbm,
    out_tok, out_route, og, ou, od,
    tok_v, cot_v, wgu, down_v, pall, send, recv, pad, xs, dgu, hid,
    dother, crecv, dacc, rs, r1, r2, send2, q1, q2, fin, ret, home, gp, gq, gsum, gall, gt,
    in_sem, z_send, z_recv, s1, n1, s2, n2, ps, pn,
    cs, cn, rs_send, rs_recv, qs, qn, fs, fn, gs, gn, hs, hn,
):
    ep, t = lax.axis_index("ep"), lax.axis_index("tp")
    z, c = ep // 2, ep % 2
    y, x = t // SIDE, t % SIDE
    p1, p2 = x + c * (y - x), y + c * (x - y)
    w1, w2 = 1 + 3 * c, 4 - 3 * c

    def block(o1, o2):
        return w1 * ((p1 + o1) % SIDE) + w2 * ((p2 + o2) % SIDE)

    def block_of_partner(o1, o2):
        return w2 * ((p2 + o1) % SIDE) + w1 * ((p1 + o2) % SIDE)

    def along1(o):
        return (ep, block(o, 0))

    def along2(o):
        return (ep, block(0, o))

    partner = (z * 2 + 1 - c, t)

    def remote(src, dst, send_sem, recv_sem, device):
        return pltpu.make_async_remote_copy(
            src_ref=src, dst_ref=dst, send_sem=send_sem, recv_sem=recv_sem,
            device_id=device, device_id_type=MESH,
        )

    scope = []

    def phase(name):
        if scope:
            scope.pop().__exit__(None, None, None)
        if name:
            scope.append(jax.named_scope(name))
            scope[0].__enter__()

    phase("greet")
    barrier = pltpu.get_barrier_semaphore()

    def greet(i, carry):
        pl.semaphore_signal(barrier, inc=1, device_id=((ep + i) % (2 * NZ), t), device_id_type=MESH)
        return carry

    def greet_plane(i, carry):
        to = (ep, (t + i) % (SIDE * SIDE))
        pl.semaphore_signal(barrier, inc=1, device_id=to, device_id_type=MESH)
        return carry

    lax.fori_loop(1, 2 * NZ, greet, 0)
    lax.fori_loop(1, SIDE * SIDE, greet_plane, 0)

    own_cols = pl.ds(pl.multiple_of(t * LANES, LANES), LANES)
    loads = [
        pltpu.make_async_copy(tok_hbm.at[:, own_cols], tok_v, in_sem.at[0]),
        pltpu.make_async_copy(cot_hbm.at[:, own_cols], cot_v, in_sem.at[1]),
        pltpu.make_async_copy(gate_hbm.at[0], wgu.at[:, pl.ds(0, LANES)], in_sem.at[2]),
        pltpu.make_async_copy(up_hbm.at[0], wgu.at[:, pl.ds(LANES, LANES)], in_sem.at[3]),
        pltpu.make_async_copy(down_hbm.at[0], down_v, in_sem.at[4]),
    ]
    for load in loads:
        load.start()

    phase("slots")
    places = lax.broadcasted_iota(jnp.int32, (NZ, LANES), 0)
    experts = (z + away(places) + NZ) % NZ
    hit0, hit1 = experts == routes[0:1, :], experts == routes[1:2, :]
    named = jnp.logical_or(hit0, hit1)
    earlier_than = (
        lax.broadcasted_iota(jnp.int32, (LANES, LANES), 0)
        < lax.broadcasted_iota(jnp.int32, (LANES, LANES), 1)
    ).astype(BF16)
    earlier = dot(named.astype(F32).astype(BF16), earlier_than, (1, 0))
    place = jnp.where(named, earlier, -1.0)
    weight = jnp.where(hit0, weights[0:1, :], 0.0) + jnp.where(hit1, weights[1:2, :], 0.0)
    slot_ids = lax.broadcasted_iota(jnp.int32, (PAD, LANES), 0).astype(F32)
    gains = []
    for j in range(NZ):
        picked = slot_ids == place[j : j + 1, :]
        pall[PAD * j : PAD * (j + 1), :] = picked.astype(F32).astype(BF16)
        gains.append(
            jnp.sum(jnp.where(picked, weight[j : j + 1, :], 0.0), axis=1, keepdims=True)
        )
    pad[...] = jnp.zeros_like(pad)
    home[...] = jnp.zeros_like(home)
    gp[...] = jnp.zeros_like(gp)
    phase("fill")
    loads[0].wait()
    rows = dot(pall[...], tok_v[...], (1, 0)).astype(BF16)
    for j in range(NZ):
        send[0, j] = rows[PAD * j : PAD * j + CAP, :]
    loads[1].wait()
    rows = dot(pall[...], cot_v[...], (1, 0))
    for j in range(NZ):
        send[1, j] = (rows[PAD * j : PAD * j + CAP, :] * gains[j][:CAP, :]).astype(BF16)
    lanes_of = lax.broadcasted_iota(jnp.int32, (HALF, NEAR * PAD), 1)
    slot = lanes_of % PAD
    squeeze = jnp.logical_and(
        lax.broadcasted_iota(jnp.int32, (HALF, NEAR * PAD), 0) == (lanes_of // PAD) * CAP + slot,
        slot < CAP,
    ).astype(F32).astype(BF16)
    for load in loads[2:]:
        load.wait()

    phase("barrier_wait")
    pl.semaphore_wait(barrier, 2 * NZ - 1 + SIDE * SIDE - 1)

    phase("dispatch")
    def to_same(j):
        i = c * NZ + j
        to = (z + away(j) + NZ) % NZ * 2 + c
        return remote(send.at[c, j], recv.at[i], z_send.at[0, j], z_recv.at[i], (to, t))

    def to_other(j):
        i = c * NZ + j
        to = (z + away(j) + NZ) % NZ * 2 + 1 - c
        return remote(send.at[1 - c, j], recv.at[i], z_send.at[1, j], z_recv.at[i], (to, t))

    def dispatch(j, carry):
        to_same(j).start()
        to_other(j).start()
        return carry

    lax.fori_loop(*OTHERS, dispatch, 0)
    to_other(SELF).start()
    recv[c * NZ + SELF] = send[c, SELF]

    waits = []

    def arrived(i):
        remote(recv.at[i], recv.at[i], z_send.at[0, 0], z_recv.at[i], partner).wait_recv()

    def arrive_one(j, carry):
        arrived(j)
        arrived(NZ + j)
        return carry

    def arrive(k):
        first, last = max(k * NEAR, OTHERS[0]), min((k + 1) * NEAR, OTHERS[1])
        lax.fori_loop(first, last, arrive_one, 0)
        if SELF // NEAR == k:
            arrived((1 - c) * NZ + SELF)
        for core in range(2):
            first = core * NZ + k * NEAR
            for i in range(first, first + NEAR):
                pad[PAD * i : PAD * i + CAP, :] = recv[i]
            at = k * PART + core * HALF
            xs[c, at : at + HALF, own_cols] = dot(
                squeeze, pad[PAD * first : PAD * (first + NEAR), :], (1, 0)
            ).astype(BF16)

    WHOLE, LOW, HIGH = (0, PART), (0, HALF), (HALF, HALF)

    def piece(k, o1, o2, part):
        cols = pl.ds(pl.multiple_of(block(o1, o2) * LANES, LANES), LANES)
        return xs.at[c, pl.ds(k * PART + part[0], part[1]), cols]

    def ship(src, dst, send_sem, recv_sem, device):
        copy = remote(src, dst, send_sem, recv_sem, device)
        copy.start()
        waits.append(copy)
        return copy

    def pass_on(k, o1, o2, part, send_sem, recv_sem, device):
        ref = piece(k, o1, o2, part)
        ship(ref, ref, send_sem, recv_sem, device)

    def came(k, o1, o2, part, recv_sem):
        ref = piece(k, o1, o2, part)
        remote(ref, ref, recv_sem, recv_sem, partner).wait_recv()

    def hand_over(k, o1, o2):
        i = (o1 % SIDE) * SIDE + o2 % SIDE
        pass_on(k, o1, o2, WHOLE, ps.at[k, i], pn.at[k, i], partner)

    def both_ways(k, o1):
        j = o1 % SIDE
        pass_on(k, o1, 0, WHOLE, s2.at[k, j, 0], n2.at[k, j, 0], along2(1))
        pass_on(k, o1, 0, WHOLE, s2.at[k, j, 1], n2.at[k, j, 1], along2(-1))

    def gather0(k):
        pass_on(k, 0, 0, WHOLE, s1.at[k, 0], n1.at[k, 0], along1(1))
        pass_on(k, 0, 0, WHOLE, s1.at[k, 1], n1.at[k, 1], along1(-1))
        both_ways(k, 0)
        hand_over(k, 0, 0)

    def gather1(k):
        came(k, -1, 0, WHOLE, n1.at[k, 0])
        pass_on(k, -1, 0, LOW, s1.at[k, 2], n1.at[k, 2], along1(1))
        both_ways(k, -1)
        hand_over(k, -1, 0)
        came(k, 1, 0, WHOLE, n1.at[k, 1])
        pass_on(k, 1, 0, HIGH, s1.at[k, 3], n1.at[k, 3], along1(-1))
        both_ways(k, 1)
        hand_over(k, 1, 0)

    def across(k, o1):
        j = o1 % SIDE
        came(k, o1, -1, WHOLE, n2.at[k, j, 0])
        pass_on(k, o1, -1, LOW, s2.at[k, j, 2], n2.at[k, j, 2], along2(1))
        hand_over(k, o1, -1)
        came(k, o1, 1, WHOLE, n2.at[k, j, 1])
        pass_on(k, o1, 1, HIGH, s2.at[k, j, 3], n2.at[k, j, 3], along2(-1))
        hand_over(k, o1, 1)

    def gather2(k):
        across(k, 0)

    def gather3(k):
        came(k, 2, 0, LOW, n1.at[k, 2])
        came(k, 2, 0, HIGH, n1.at[k, 3])
        both_ways(k, 2)
        hand_over(k, 2, 0)

    def gather4(k):
        across(k, -1)
        across(k, 1)

    def gather5(k):
        across(k, 2)

    def last_of(k, o1):
        j = o1 % SIDE
        came(k, o1, 2, LOW, n2.at[k, j, 2])
        came(k, o1, 2, HIGH, n2.at[k, j, 3])
        hand_over(k, o1, 2)

    def gather6(k):
        for o1 in (0, -1, 1, 2):
            last_of(k, o1)

    def gather7(k):
        for o1 in range(SIDE):
            for o2 in range(SIDE):
                cols = pl.ds(pl.multiple_of(block_of_partner(o1, o2) * LANES, LANES), LANES)
                ref = xs.at[1 - c, pl.ds(k * PART, PART), cols]
                sem = pn.at[k, o1 * SIDE + o2]
                remote(ref, ref, sem, sem, partner).wait_recv()

    combine = {}
    order = (2, 1, 3, 0)

    def expert(k):
        at = slice(k * PART, (k + 1) * PART)
        pre = dot(xs[0, at, :], wgu[...], (1, 0))
        dh = dot(xs[1, at, :], down_v[...], (1, 1))
        a, b = pre[:, :LANES], pre[:, LANES:]
        sigma = jax.nn.sigmoid(a)
        activ = a * sigma
        hidden = activ * b
        dgu[at, :LANES] = (dh * b * sigma * (1.0 + a * (1.0 - sigma))).astype(BF16)
        dgu[at, LANES:] = (dh * activ).astype(BF16)
        hid[at, :] = hidden.astype(BF16)
        part = hidden * dh
        high = part.astype(BF16)
        low = (part - high.astype(F32)).astype(BF16)
        for core in range(2):
            here = slice(core * HALF, (core + 1) * HALF)
            units = dot(high[here, :], squeeze, (0, 0)) + dot(low[here, :], squeeze, (0, 0))
            line = jnp.sum(units, axis=0, keepdims=True)
            for i in range(GATES):
                gp[k, core * GATES + i : core * GATES + i + 1, :] = line[
                    :, LANES * i : LANES * (i + 1)
                ]

    gates = {}

    def gate0(k):
        gates[k] = ship(gp.at[k], gq.at[k], gs.at[k], gn.at[k], partner)

    def gate1(k):
        gates[k].wait_recv()
        gsum[k] = gp[k] + gq[k]
        gates[k] = []
        for i in range(1, SIDE * SIDE):
            to = (ep, block(i // SIDE, i % SIDE))
            gates[k].append(
                ship(gsum.at[k], gall.at[k, i - 1], hs.at[k, i - 1], hn.at[k, i - 1], to)
            )

    def gate2(k):
        for copy in gates[k]:
            copy.wait_recv()
        total = gsum[k]
        for i in range(SIDE * SIDE - 1):
            total = total + gall[k, i]
        gt[k] = total

    def dx_other(k):
        rows_of = pl.ds(pl.multiple_of(k * PART + (1 - c) * HALF, 8), HALF)
        for o1 in order:
            for o2 in range(SIDE):
                units = pl.ds(pl.multiple_of(block_of_partner(o1, o2) * LANES, LANES), LANES)
                dother[k, o1, o2] = dot(dgu[rows_of, :], wgu[units, :], (1, 1)).astype(BF16)
            combine[k, o1] = ship(
                dother.at[k, o1], crecv.at[k, o1], cs.at[k, o1], cn.at[k, o1], partner
            )

    def dx_own(k):
        rows_of = pl.ds(pl.multiple_of(k * PART + c * HALF, 8), HALF)
        for o1 in order:
            for o2 in range(SIDE):
                units = pl.ds(pl.multiple_of(block(o1, o2) * LANES, LANES), LANES)
                dacc[k, o1, o2] = dot(dgu[rows_of, :], wgu[units, :], (1, 1))

    lo, hi = pl.ds(0, CUT), pl.ds(CUT, HALF - CUT)
    flight = {}

    def both(k, o1, part):
        return dacc[k, o1, :, part] + crecv[k, o1, :, part].astype(F32)

    def scatter1(k):
        ss, rr = rs_send.at[k], rs_recv.at[k]
        combine[k, 2].wait_recv()
        rs[k, 2] = (dacc[k, 2] + crecv[k, 2].astype(F32)).astype(BF16)
        flight[k, 0] = ship(
            rs.at[k, 2, :, lo], r1.at[k, 0, :, lo], ss.at[0], rr.at[0], along1(1)
        )
        flight[k, 1] = ship(
            rs.at[k, 2, :, hi], r1.at[k, 1, :, hi], ss.at[1], rr.at[1], along1(-1)
        )
        combine[k, 1].wait_recv()
        rs[k, 1, :, hi] = both(k, 1, hi).astype(BF16)
        flight[k, 2] = ship(
            rs.at[k, 1, :, hi], r2.at[k, 0, :, hi], ss.at[2], rr.at[2], along1(1)
        )
        combine[k, 3].wait_recv()
        rs[k, 3, :, lo] = both(k, 3, lo).astype(BF16)
        flight[k, 3] = ship(
            rs.at[k, 3, :, lo], r2.at[k, 1, :, lo], ss.at[3], rr.at[3], along1(-1)
        )

    def scatter2(k):
        ss, rr = rs_send.at[k], rs_recv.at[k]
        flight[k, 0].wait_recv()
        rs[k, 1, :, lo] = (both(k, 1, lo) + r1[k, 0, :, lo].astype(F32)).astype(BF16)
        flight[k, 4] = ship(
            rs.at[k, 1, :, lo], r2.at[k, 0, :, lo], ss.at[4], rr.at[4], along1(1)
        )
        flight[k, 1].wait_recv()
        rs[k, 3, :, hi] = (both(k, 3, hi) + r1[k, 1, :, hi].astype(F32)).astype(BF16)
        flight[k, 5] = ship(
            rs.at[k, 3, :, hi], r2.at[k, 1, :, hi], ss.at[5], rr.at[5], along1(-1)
        )

    def scatter3(k):
        ss, rr = qs.at[k], qn.at[k]
        combine[k, 0].wait_recv()
        for i in (2, 3, 4, 5):
            flight[k, i].wait_recv()

        def summed(o2):
            return (
                dacc[k, 0, o2] + crecv[k, 0, o2].astype(F32)
                + r2[k, 0, o2].astype(F32) + r2[k, 1, o2].astype(F32)
            )

        send2[k, 2] = summed(2).astype(BF16)
        flight[k, 0] = ship(send2.at[k, 2, lo], q1.at[k, 0, lo], ss.at[0], rr.at[0], along2(1))
        flight[k, 1] = ship(send2.at[k, 2, hi], q1.at[k, 1, hi], ss.at[1], rr.at[1], along2(-1))
        dacc[k, 0, 1] = summed(1)
        send2[k, 1, hi] = dacc[k, 0, 1, hi].astype(BF16)
        flight[k, 2] = ship(send2.at[k, 1, hi], q2.at[k, 0, hi], ss.at[2], rr.at[2], along2(1))
        dacc[k, 0, 3] = summed(3)
        send2[k, 3, lo] = dacc[k, 0, 3, lo].astype(BF16)
        flight[k, 3] = ship(send2.at[k, 3, lo], q2.at[k, 1, lo], ss.at[3], rr.at[3], along2(-1))
        dacc[k, 0, 0] = summed(0)

    def scatter4(k):
        ss, rr = qs.at[k], qn.at[k]
        flight[k, 0].wait_recv()
        send2[k, 1, lo] = (dacc[k, 0, 1, lo] + q1[k, 0, lo].astype(F32)).astype(BF16)
        flight[k, 4] = ship(send2.at[k, 1, lo], q2.at[k, 0, lo], ss.at[4], rr.at[4], along2(1))
        flight[k, 1].wait_recv()
        send2[k, 3, hi] = (dacc[k, 0, 3, hi] + q1[k, 1, hi].astype(F32)).astype(BF16)
        flight[k, 5] = ship(send2.at[k, 3, hi], q2.at[k, 1, hi], ss.at[5], rr.at[5], along2(-1))

    def home_of(j):
        to = (z - away(j) + NZ) % NZ * 2 + c
        return remote(fin.at[j], ret.at[j], fs.at[j], fn.at[j], (to, t))

    def go_home(j, carry):
        home_of(j).start()
        return carry

    def scatter5(k):
        for i in (2, 3, 4, 5):
            flight[k, i].wait_recv()
        total = dacc[k, 0, 0] + q2[k, 0].astype(F32) + q2[k, 1].astype(F32)
        spread = dot(squeeze, total.astype(BF16), (0, 0))
        below = lax.broadcasted_iota(jnp.int32, (PAD, LANES), 0) >= CAP
        for i in range(NEAR):
            r = i * PAD // LANES
            line = jnp.where(c == 0, gt[k, r : r + 1, :], gt[k, GATES + r : GATES + r + 1, :])
            fin[k * NEAR + i] = jnp.where(below, line, spread[PAD * i : PAD * (i + 1), :])[
                :BACK, :
            ].astype(BF16)
        first, last = max(k * NEAR, OTHERS[0]), min((k + 1) * NEAR, OTHERS[1])
        lax.fori_loop(first, last, go_home, 0)
        if SELF // NEAR == k:
            ret[SELF] = fin[SELF]

    def grads(k, carry):
        cols = pl.ds(pl.multiple_of(k * 256, 256), 256)
        part = dot(xs[0, :, cols], dgu[...], (0, 0))
        og[0, cols, :] = part[:, :LANES].astype(BF16)
        ou[0, cols, :] = part[:, LANES:].astype(BF16)
        return carry

    def unit_grads(k):
        lax.fori_loop(0, MODEL // 256, grads, 0)

    def down_grads(k):
        od[0] = dot(hid[...], xs[1], (0, 0)).astype(BF16)

    stages = dict(
        arrive=arrive, gather0=gather0, gather1=gather1, gather2=gather2, gather3=gather3,
        gather4=gather4, gather5=gather5, gather6=gather6, gather7=gather7, expert=expert,
        gate0=gate0, gate1=gate1, gate2=gate2, dx_other=dx_other, dx_own=dx_own,
        scatter1=scatter1, scatter2=scatter2, scatter3=scatter3, scatter4=scatter4,
        scatter5=scatter5, unit_grads=unit_grads, down_grads=down_grads,
    )
    for entry in SCHEDULE:
        phase(entry)
        stages[entry[:-1]](int(entry[-1]))

    phase("rows_came")

    def rows_came(j, carry):
        home_of(j).wait_recv()
        return carry

    lax.fori_loop(*OTHERS, rows_came, 0)
    phase("home")
    for j in range(NZ):
        home[j, :BACK, :] = ret[j]
    flat = home[...].reshape(NZ * PAD, LANES)
    out_tok[...] = dot(pall[...], flat, (0, 0)).astype(BF16)
    at_j = lax.broadcasted_iota(jnp.int32, (NZ, NZ * PAD), 0)
    at_row = lax.broadcasted_iota(jnp.int32, (NZ, NZ * PAD), 1)
    lines = dot((at_row == PAD * at_j + CAP).astype(F32).astype(BF16), flat, (1, 0))
    lines = jnp.concatenate([lines] * (NZ * PAD // LANES), axis=1)
    lines = jnp.where(at_row // PAD == at_j, lines, 0.0).astype(BF16)
    values = dot(lines, pall[...], (1, 0))
    for i, hit in enumerate((hit0, hit1)):
        out_route[i : i + 1, :] = (
            jnp.sum(jnp.where(hit, values, 0.0), axis=0, keepdims=True) / weights[i : i + 1, :]
        )

    phase("drain")
    def drain(j, carry):
        to_same(j).wait_send()
        to_other(j).wait_send()
        home_of(j).wait_send()
        return carry

    lax.fori_loop(*OTHERS, drain, 0)
    to_other(SELF).wait_send()
    for copy in waits:
        copy.wait_send()
    phase(None)


def store(*refs):
    n = len(refs) // 2
    copies = [
        pltpu.make_async_copy(refs[i], refs[n + i], refs[-1].at[i]) for i in range(n)
    ]
    for copy in copies:
        copy.start()
    for copy in copies:
        copy.wait()


def local(tokens, routes, route_weights, out_grad, gate_proj, up_proj, down_proj):
    vmem, hbm = pl.BlockSpec(memory_space=pltpu.VMEM), pl.BlockSpec(memory_space=pl.ANY)
    dma, buf = pltpu.SemaphoreType.DMA, pltpu.VMEM
    quad = (SIDE, HALF, LANES)
    shapes = [
        ((LANES, LANES), BF16),
        ((2, LANES), F32),
        ((1, MODEL, LANES), BF16),
        ((1, MODEL, LANES), BF16),
        ((1, LANES, MODEL), BF16),
    ]
    out = pl.pallas_call(
        kernel,
        out_shape=tuple(pltpu.VMEM(*s) for s in shapes),
        in_specs=[vmem, vmem, hbm, hbm, hbm, hbm, hbm],
        out_specs=[vmem] * 5,
        scratch_shapes=[
            buf((LANES, LANES), BF16),
            buf((LANES, LANES), BF16),
            buf((MODEL, 2 * LANES), BF16),
            buf((LANES, MODEL), BF16),
            buf((NZ * PAD, LANES), BF16),
            buf((2, NZ, CAP, LANES), BF16),
            buf((2 * NZ, CAP, LANES), BF16),
            buf((2 * NZ * PAD, LANES), BF16),
            buf((2, ROWS, MODEL), BF16),
            buf((ROWS, 2 * LANES), BF16),
            buf((ROWS, LANES), BF16),
            buf((CHUNKS, SIDE, *quad), BF16),
            buf((CHUNKS, SIDE, *quad), BF16),
            buf((CHUNKS, SIDE, *quad), F32),
            buf((CHUNKS, SIDE, *quad), BF16),
            buf((CHUNKS, 2, *quad), BF16),
            buf((CHUNKS, 2, *quad), BF16),
            buf((CHUNKS, *quad), BF16),
            buf((CHUNKS, 2, HALF, LANES), BF16),
            buf((CHUNKS, 2, HALF, LANES), BF16),
            buf((NZ, BACK, LANES), BF16),
            buf((NZ, BACK, LANES), BF16),
            buf((NZ, PAD, LANES), BF16),
            buf((CHUNKS, 8, LANES), F32),
            buf((CHUNKS, 8, LANES), F32),
            buf((CHUNKS, 8, LANES), F32),
            buf((CHUNKS, SIDE * SIDE - 1, 8, LANES), F32),
            buf((CHUNKS, 8, LANES), F32),
            dma((5,)),
            dma((2, NZ)),
            dma((2 * NZ,)),
            dma((CHUNKS, 4)),
            dma((CHUNKS, 4)),
            dma((CHUNKS, SIDE, 4)),
            dma((CHUNKS, SIDE, 4)),
            dma((CHUNKS, SIDE * SIDE)),
            dma((CHUNKS, SIDE * SIDE)),
            dma((CHUNKS, SIDE)),
            dma((CHUNKS, SIDE)),
            dma((CHUNKS, 6)),
            dma((CHUNKS, 6)),
            dma((CHUNKS, 6)),
            dma((CHUNKS, 6)),
            dma((NZ,)),
            dma((NZ,)),
            dma((CHUNKS,)),
            dma((CHUNKS,)),
            dma((CHUNKS, SIDE * SIDE - 1)),
            dma((CHUNKS, SIDE * SIDE - 1)),
        ],
        compiler_params=pltpu.CompilerParams(
            collective_id=0, has_side_effects=True, vmem_limit_bytes=56 * 2**20
        ),
        name="routed_backward",
    )(routes.T, route_weights.T, tokens, out_grad, gate_proj, up_proj, down_proj)
    out = pl.pallas_call(
        store,
        out_shape=tuple(jax.ShapeDtypeStruct(*s) for s in shapes),
        in_specs=[vmem] * 5,
        out_specs=[hbm] * 5,
        scratch_shapes=[dma((5,))],
        name="store",
    )(*(pltpu.with_memory_space_constraint(a, pltpu.VMEM) for a in out))
    return (out[0], out[1].T, out[2], out[3], out[4])


SCHEDULE = (
    "arrive0", "gather00", "gather10", "gather20", "gather30", "gather40", "gather50",
    "gather60", "gather70", "expert0", "gate00", "dx_other0", "gate10", "dx_own0", "scatter10",
    "scatter20", "gate20", "scatter30", "scatter40", "scatter50", "unit_grads0", "down_grads0",
)


def solution(mesh):
    placed = (
        P("ep", None),
        P("ep", None),
        P("ep", None),
        P("ep", None),
        P("ep", None, "tp"),
        P("ep", None, "tp"),
        P("ep", "tp", None),
    )
    return jax.shard_map(
        local,
        mesh=mesh,
        in_specs=placed,
        out_specs=(
            P("ep", "tp"),
            P("ep", None),
            P("ep", None, "tp"),
            P("ep", None, "tp"),
            P("ep", "tp", None),
        ),
        check_vma=False,
    )
```

time: 274 us -> 80.1 us (0.29)
  the two profiles are of different devices: /device:TPU:1 before, /device:TPU:14 now
where the time goes in v2:
time: 80.1 us; the launch traced here: 80 us
  Pallas kernels  79.3 us (99%)
    pallas_call x1, Pallas kernels, local(): pl.pallas_call(kernel, out_shape=tuple((pltpu.VMEM(*s) for s in shapes)),...  78.1 us

profile of v2, /device:TPU:14, one launch (start us, length us, event | category | flops | bytes accessed | tf_op | source)
XLA Modules:
  0.0 80.0 jit_solution(5327082371558676424)
XLA Ops:
  0.6 78.1 %routed_backward.1 = (bf16[128,128]{1,0:T(8,128)(2,1)S(1)}, f32[2,128]{1,0:T(2,128)S(1)}, bf16[1,2048,128]{2,1,0:T(8,128)(2,1)S(1)}, bf16[1,2048,128]{2,1,0:T(8,128)(2,1)S(1)}, bf16[1,128,2048]{2,1,0:T(8,128)(2,1)S(1)}) custom-call(s32[2,128]{1,0:T(2,128)} %bitcast.3, f32[2,128]{1,0:T(2,128)} %bitcast.4, bf16[128,2048]{1,0:T(8,128)(2,1)} %tok_hbm.1, ...), custom_call_target="tpu_custom_call" | custom-call | tf_op jit(solution)/shard_map/routed_backward/pallas_call | solution.py:526
  78.8 1.2 %store.1 = (bf16[128,128]{1,0:T(8,128)(2,1)}, f32[2,128]{1,0:T(2,128)}, bf16[1,2048,128]{2,1,0:T(8,128)(2,1)}, bf16[1,2048,128]{2,1,0:T(8,128)(2,1)}, bf16[1,128,2048]{2,1,0:T(8,128)(2,1)}) custom-call(bf16[128,128]{1,0:T(8,128)(2,1)S(1)} %get-tuple-element.15.refs_0_, f32[2,128]{1,0:T(2,128)S(1)} %get-tuple-element.16.refs_1_, ...), custom_call_target="tpu_custom_call" | custom-call | tf_op jit(solution)/shard_map/store/pallas_call | solution.py:587

commit v3 on v2

v3 whole, which is shorter than its diff:
```python
import jax
import jax.numpy as jnp
from jax import lax
from jax.experimental import pallas as pl
from jax.experimental.pallas import tpu as pltpu
from jax.sharding import PartitionSpec as P

MESH = pl.DeviceIdType.MESH
F32, BF16 = jnp.float32, jnp.bfloat16
NZ, SIDE = 16, 4
CAP, PAD, BACK, SENT = 18, 32, 24, 40
LANES = 128
MODEL = 2048
ROWS = 2 * NZ * CAP
CHUNKS = 2
NEAR = NZ // CHUNKS
HALF = NEAR * CAP
PART = 2 * HALF
SELF, OTHERS = NZ - 1, (0, NZ - 1)
DIRECT = (2,)
GATES = NEAR * PAD // LANES


def dot(left, right, dims):
    return lax.dot_general(
        left, right, ((dims[:1], dims[1:]), ((), ())), preferred_element_type=F32
    )


def away(i):
    step = NZ // 2 - (i + 1) // 2
    return step * (2 * (i % 2) - 1)


def kernel(
    routes_hbm, weights_hbm, tok_hbm, cot_hbm, gate_hbm, up_hbm, down_hbm,
    out_tok, out_route, og, ou, od,
    routes, weights, tok_v, cot_v, wgu, wgu_t, down_v, down_t, pall, pdy, send, recv, xs, dgu, hid,
    dother, crecv, dacc, rs, r1, rs2, r2, fin, ret, home, gp, gq, gsum, gall, gt,
    in_sem, z_send, z_recv, s1, n1, s2, n2, ps, pn,
    cs, cn, rs_send, rs_recv, qs, qn, fs, fn, gs, gn, hs, hn,
):
    ep, t = lax.axis_index("ep"), lax.axis_index("tp")
    z, c = ep // 2, ep % 2
    y, x = t // SIDE, t % SIDE
    p1, p2 = x + c * (y - x), y + c * (x - y)
    w1, w2 = 1 + 3 * c, 4 - 3 * c

    def block(o1, o2):
        return w1 * ((p1 + o1) % SIDE) + w2 * ((p2 + o2) % SIDE)

    def block_of_partner(o1, o2):
        return w2 * ((p2 + o1) % SIDE) + w1 * ((p1 + o2) % SIDE)

    def along1(o):
        return (ep, block(o, 0))

    def along2(o):
        return (ep, block(0, o))

    partner = (z * 2 + 1 - c, t)

    def remote(src, dst, send_sem, recv_sem, device):
        return pltpu.make_async_remote_copy(
            src_ref=src, dst_ref=dst, send_sem=send_sem, recv_sem=recv_sem,
            device_id=device, device_id_type=MESH,
        )

    scope = []

    def phase(name):
        if scope:
            scope.pop().__exit__(None, None, None)
        if name:
            scope.append(jax.named_scope(name))
            scope[0].__enter__()

    own_cols = pl.ds(pl.multiple_of(t * LANES, LANES), LANES)
    loads = [
        pltpu.make_async_copy(routes_hbm, routes, in_sem.at[5]),
        pltpu.make_async_copy(weights_hbm, weights, in_sem.at[6]),
        pltpu.make_async_copy(tok_hbm.at[:, own_cols], tok_v, in_sem.at[0]),
        pltpu.make_async_copy(cot_hbm.at[:, own_cols], cot_v, in_sem.at[1]),
        pltpu.make_async_copy(gate_hbm.at[0], wgu.at[:, pl.ds(0, LANES)], in_sem.at[2]),
        pltpu.make_async_copy(up_hbm.at[0], wgu.at[:, pl.ds(LANES, LANES)], in_sem.at[3]),
        pltpu.make_async_copy(down_hbm.at[0], down_v, in_sem.at[4]),
    ]
    for load in loads:
        load.start()

    phase("greet")
    barrier = pltpu.get_barrier_semaphore()

    def greet(i, carry):
        to = ((ep + 2 * i) % (2 * NZ), t)
        pl.semaphore_signal(barrier, inc=1, device_id=to, device_id_type=MESH)
        return carry

    def greet_plane(i, carry):
        to = (ep, (t + i) % (SIDE * SIDE))
        pl.semaphore_signal(barrier, inc=1, device_id=to, device_id_type=MESH)
        return carry

    lax.fori_loop(1, NZ, greet, 0)
    pl.semaphore_signal(barrier, inc=1, device_id=partner, device_id_type=MESH)
    lax.fori_loop(1, SIDE * SIDE, greet_plane, 0)

    phase("slots")
    loads[0].wait()
    loads[1].wait()
    places = lax.broadcasted_iota(jnp.int32, (NZ, LANES), 0)
    experts = (z + away(places) + NZ) % NZ
    hit0, hit1 = experts == routes[0:1, :], experts == routes[1:2, :]
    named = jnp.logical_or(hit0, hit1)
    earlier_than = (
        lax.broadcasted_iota(jnp.int32, (LANES, LANES), 0)
        < lax.broadcasted_iota(jnp.int32, (LANES, LANES), 1)
    ).astype(BF16)
    earlier = dot(named.astype(F32).astype(BF16), earlier_than, (1, 0))
    place = jnp.where(named, earlier, -1.0)
    weight = jnp.where(hit0, weights[0:1, :], 0.0) + jnp.where(hit1, weights[1:2, :], 0.0)
    sent_ids = lax.broadcasted_iota(jnp.int32, (SENT, LANES), 0)
    x_ids = jnp.where(sent_ids < CAP, sent_ids, -2).astype(F32)
    dy_ids = jnp.where(sent_ids >= CAP, sent_ids - CAP, -2).astype(F32)
    gains = []
    for j in range(NZ):
        here = slice(SENT * j, SENT * (j + 1))
        pall[here, :] = (x_ids == place[j : j + 1, :]).astype(F32).astype(BF16)
        picked = dy_ids == place[j : j + 1, :]
        pdy[here, :] = picked.astype(F32).astype(BF16)
        gains.append(
            jnp.sum(jnp.where(picked, weight[j : j + 1, :], 0.0), axis=1, keepdims=True)
        )
    home[...] = jnp.zeros_like(home)
    gp[...] = jnp.zeros_like(gp)
    phase("fill")
    loads[2].wait()
    loads[3].wait()
    x_sent = dot(pall[...], tok_v[...], (1, 0))
    dy_sent = dot(pdy[...], cot_v[...], (1, 0))
    for j in range(NZ):
        here = slice(SENT * j, SENT * (j + 1))
        send[here, :] = (x_sent[here, :] + dy_sent[here, :] * gains[j]).astype(BF16)
    row_of = lax.broadcasted_iota(jnp.int32, (HALF, NEAR * SENT), 0)
    lanes_of = lax.broadcasted_iota(jnp.int32, (HALF, NEAR * SENT), 1)
    from_row = lanes_of % SENT
    at_row = (lanes_of // SENT) * CAP + from_row
    pick_x = jnp.logical_and(row_of == at_row, from_row < CAP).astype(F32).astype(BF16)
    pick_dy = jnp.logical_and(
        row_of == at_row - CAP, jnp.logical_and(from_row >= CAP, from_row < 2 * CAP)
    ).astype(F32).astype(BF16)
    lanes_of = lax.broadcasted_iota(jnp.int32, (HALF, NEAR * PAD), 1)
    slot = lanes_of % PAD
    squeeze = jnp.logical_and(
        lax.broadcasted_iota(jnp.int32, (HALF, NEAR * PAD), 0) == (lanes_of // PAD) * CAP + slot,
        slot < CAP,
    ).astype(F32).astype(BF16)
    phase("barrier_wait")
    pl.semaphore_wait(barrier, NZ + SIDE * SIDE - 1)

    phase("dispatch")
    def sent(j):
        return pl.ds(pl.multiple_of(j * SENT, 8), SENT)

    def to_expert(j):
        to = (z + away(j) + NZ) % NZ * 2 + c
        return remote(send.at[sent(j), :], recv.at[sent(j), :], z_send.at[j], z_recv.at[j], (to, t))

    def dispatch(j, carry):
        to_expert(j).start()
        return carry

    lax.fori_loop(*OTHERS, dispatch, 0)
    recv[SENT * SELF : SENT * (SELF + 1), :] = send[SENT * SELF : SENT * (SELF + 1), :]

    waits = []

    phase("turn")
    for load in loads[4:]:
        load.wait()
    for i in range(SIDE * SIDE):
        at = slice(LANES * i, LANES * (i + 1))
        wgu_t[i] = wgu[at, :].T
        down_t[at, :] = down_v[:, at].T

    def arrive_one(j, carry):
        to_expert(j).wait_recv()
        return carry

    def arrive(k):
        first, last = max(k * NEAR, OTHERS[0]), min((k + 1) * NEAR, OTHERS[1])
        lax.fori_loop(first, last, arrive_one, 0)
        came_in = recv[SENT * NEAR * k : SENT * NEAR * (k + 1), :]
        at = pl.ds(pl.multiple_of(k * PART + c * HALF, 8), HALF)
        xs[0, at, own_cols] = dot(pick_x, came_in, (1, 0)).astype(BF16)
        xs[1, at, own_cols] = dot(pick_dy, came_in, (1, 0)).astype(BF16)

    WHOLE, LOW, HIGH = (0, 2), (0, 1), (1, 1)

    def piece(k, o1, o2, part):
        cols = pl.ds(pl.multiple_of(block(o1, o2) * LANES, LANES), LANES)
        at = pl.ds(pl.multiple_of(k * PART + c * HALF, 8), HALF)
        return xs.at[pl.ds(*part), at, cols]

    def ship(src, dst, send_sem, recv_sem, device):
        copy = remote(src, dst, send_sem, recv_sem, device)
        copy.start()
        waits.append(copy)
        return copy

    def pass_on(k, o1, o2, part, send_sem, recv_sem, device):
        ref = piece(k, o1, o2, part)
        ship(ref, ref, send_sem, recv_sem, device)

    def came(k, o1, o2, part, recv_sem):
        ref = piece(k, o1, o2, part)
        remote(ref, ref, recv_sem, recv_sem, partner).wait_recv()

    def hand_over(k, o1, o2):
        i = (o1 % SIDE) * SIDE + o2 % SIDE
        pass_on(k, o1, o2, WHOLE, ps.at[k, i], pn.at[k, i], partner)

    def both_ways(k, o1):
        j = o1 % SIDE
        pass_on(k, o1, 0, WHOLE, s2.at[k, j, 0], n2.at[k, j, 0], along2(1))
        pass_on(k, o1, 0, WHOLE, s2.at[k, j, 1], n2.at[k, j, 1], along2(-1))
        if j in DIRECT:
            pass_on(k, o1, 0, WHOLE, s2.at[k, j, 2], n2.at[k, j, 2], along2(2))

    def gather0(k):
        pass_on(k, 0, 0, WHOLE, s1.at[k, 0], n1.at[k, 0], along1(1))
        pass_on(k, 0, 0, WHOLE, s1.at[k, 1], n1.at[k, 1], along1(-1))
        pass_on(k, 0, 0, WHOLE, s1.at[k, 2], n1.at[k, 2], along1(2))
        both_ways(k, 0)
        hand_over(k, 0, 0)

    def gather1(k):
        came(k, -1, 0, WHOLE, n1.at[k, 0])
        both_ways(k, -1)
        hand_over(k, -1, 0)
        came(k, 1, 0, WHOLE, n1.at[k, 1])
        both_ways(k, 1)
        hand_over(k, 1, 0)

    def across(k, o1):
        j = o1 % SIDE
        came(k, o1, -1, WHOLE, n2.at[k, j, 0])
        if j not in DIRECT:
            pass_on(k, o1, -1, LOW, s2.at[k, j, 2], n2.at[k, j, 2], along2(1))
        hand_over(k, o1, -1)
        came(k, o1, 1, WHOLE, n2.at[k, j, 1])
        if j not in DIRECT:
            pass_on(k, o1, 1, HIGH, s2.at[k, j, 3], n2.at[k, j, 3], along2(-1))
        hand_over(k, o1, 1)

    def gather2(k):
        across(k, 0)

    def gather3(k):
        came(k, 2, 0, WHOLE, n1.at[k, 2])
        both_ways(k, 2)
        hand_over(k, 2, 0)

    def gather4(k):
        across(k, -1)
        across(k, 1)

    def gather5(k):
        across(k, 2)

    def last_of(k, o1):
        j = o1 % SIDE
        if j in DIRECT:
            came(k, o1, 2, WHOLE, n2.at[k, j, 2])
        else:
            came(k, o1, 2, LOW, n2.at[k, j, 2])
            came(k, o1, 2, HIGH, n2.at[k, j, 3])
        hand_over(k, o1, 2)

    def gather6(k):
        for o1 in (0, -1, 1, 2):
            last_of(k, o1)

    def gather7(k):
        for o1 in range(SIDE):
            for o2 in range(SIDE):
                cols = pl.ds(pl.multiple_of(block_of_partner(o1, o2) * LANES, LANES), LANES)
                at = pl.ds(pl.multiple_of(k * PART + (1 - c) * HALF, 8), HALF)
                ref = xs.at[:, at, cols]
                sem = pn.at[k, o1 * SIDE + o2]
                remote(ref, ref, sem, sem, partner).wait_recv()

    combine = {}
    order = (2, 1, 3, 0)

    def expert(k):
        at = slice(k * PART, (k + 1) * PART)
        pre = dot(xs[0, at, :], wgu[...], (1, 0))
        dh = dot(xs[1, at, :], down_t[...], (1, 0))
        a, b = pre[:, :LANES], pre[:, LANES:]
        sigma = jax.nn.sigmoid(a)
        activ = a * sigma
        hidden = activ * b
        dgu[at, :LANES] = (dh * b * sigma * (1.0 + a * (1.0 - sigma))).astype(BF16)
        dgu[at, LANES:] = (dh * activ).astype(BF16)
        hid[at, :] = hidden.astype(BF16)
        part = hidden * dh
        high = part.astype(BF16)
        low = (part - high.astype(F32)).astype(BF16)
        for core in range(2):
            here = slice(core * HALF, (core + 1) * HALF)
            units = dot(high[here, :], squeeze, (0, 0)) + dot(low[here, :], squeeze, (0, 0))
            line = jnp.sum(units, axis=0, keepdims=True)
            for i in range(GATES):
                gp[k, core * GATES + i : core * GATES + i + 1, :] = line[
                    :, LANES * i : LANES * (i + 1)
                ]

    gates = {}

    def gate0(k):
        gates[k] = ship(gp.at[k], gq.at[k], gs.at[k], gn.at[k], partner)

    def gate1(k):
        gates[k].wait_recv()
        gsum[k] = gp[k] + gq[k]
        gates[k] = []
        for i in range(1, SIDE * SIDE):
            to = (ep, block(i // SIDE, i % SIDE))
            gates[k].append(
                ship(gsum.at[k], gall.at[k, i - 1], hs.at[k, i - 1], hn.at[k, i - 1], to)
            )

    def gate2(k):
        for copy in gates[k]:
            copy.wait_recv()
        total = gsum[k]
        for i in range(SIDE * SIDE - 1):
            total = total + gall[k, i]
        gt[k] = total

    def dx_other(k):
        rows_of = pl.ds(pl.multiple_of(k * PART + (1 - c) * HALF, 8), HALF)
        for o1 in order:
            for o2 in range(SIDE):
                units = wgu_t[block_of_partner(o1, o2)]
                dother[k, o1, o2] = dot(dgu[rows_of, :], units, (1, 0)).astype(BF16)
            combine[k, o1] = ship(
                dother.at[k, o1], crecv.at[k, o1], cs.at[k, o1], cn.at[k, o1], partner
            )

    def partial(k, o1, o2):
        rows_of = pl.ds(pl.multiple_of(k * PART + c * HALF, 8), HALF)
        return dot(dgu[rows_of, :], wgu_t[block(o1, o2)], (1, 0))

    flight = {}

    def scatter1(k):
        for o1 in order:
            for o2 in range(SIDE):
                dacc[k, o1, o2] = partial(k, o1, o2)
            if o1:
                combine[k, o1].wait_recv()
                rs[k, o1] = (dacc[k, o1] + crecv[k, o1].astype(F32)).astype(BF16)
                flight[k, o1] = ship(
                    rs.at[k, o1], r1.at[k, o1 - 1], rs_send.at[k, o1], rs_recv.at[k, o1], along1(o1)
                )

    def scatter2(k):
        combine[k, 0].wait_recv()
        for o1 in (1, 3, 2):
            flight[k, o1].wait_recv()
        for o2 in order:
            total = (
                dacc[k, 0, o2] + crecv[k, 0, o2].astype(F32)
                + r1[k, 0, o2].astype(F32) + r1[k, 1, o2].astype(F32) + r1[k, 2, o2].astype(F32)
            )
            if o2:
                rs2[k, o2] = total.astype(BF16)
                flight[k, o2] = ship(
                    rs2.at[k, o2], r2.at[k, o2 - 1], qs.at[k, o2], qn.at[k, o2], along2(o2)
                )
            else:
                dacc[k, 0, 0] = total

    def home_of(j):
        to = (z - away(j) + NZ) % NZ * 2 + c
        return remote(fin.at[j], ret.at[j], fs.at[j], fn.at[j], (to, t))

    def go_home(j, carry):
        home_of(j).start()
        return carry

    def scatter3(k):
        for o2 in (1, 3, 2):
            flight[k, o2].wait_recv()
        total = (
            dacc[k, 0, 0] + r2[k, 0].astype(F32) + r2[k, 1].astype(F32) + r2[k, 2].astype(F32)
        )
        spread = dot(squeeze, total.astype(BF16), (0, 0))
        below = lax.broadcasted_iota(jnp.int32, (PAD, LANES), 0) >= CAP
        for i in range(NEAR):
            r = i * PAD // LANES
            line = jnp.where(c == 0, gt[k, r : r + 1, :], gt[k, GATES + r : GATES + r + 1, :])
            fin[k * NEAR + i] = jnp.where(below, line, spread[PAD * i : PAD * (i + 1), :])[
                :BACK, :
            ].astype(BF16)
        first, last = max(k * NEAR, OTHERS[0]), min((k + 1) * NEAR, OTHERS[1])
        lax.fori_loop(first, last, go_home, 0)
        if SELF // NEAR == k:
            ret[SELF] = fin[SELF]

    def grads(k, carry):
        cols = pl.ds(pl.multiple_of(k * 256, 256), 256)
        part = dot(xs[0, :, cols], dgu[...], (0, 0))
        og[0, cols, :] = part[:, :LANES].astype(BF16)
        ou[0, cols, :] = part[:, LANES:].astype(BF16)
        return carry

    def unit_grads(k):
        lax.fori_loop(0, MODEL // 256, grads, 0)

    def down_grads(k):
        od[0] = dot(hid[...], xs[1], (0, 0)).astype(BF16)

    stages = dict(
        arrive=arrive, gather0=gather0, gather1=gather1, gather2=gather2, gather3=gather3,
        gather4=gather4, gather5=gather5, gather6=gather6, gather7=gather7, expert=expert,
        gate0=gate0, gate1=gate1, gate2=gate2, dx_other=dx_other, scatter1=scatter1,
        scatter2=scatter2, scatter3=scatter3, unit_grads=unit_grads, down_grads=down_grads,
    )
    for entry in SCHEDULE:
        phase(entry)
        stages[entry[:-1]](int(entry[-1]))

    phase("rows_came")

    def rows_came(j, carry):
        home_of(j).wait_recv()
        return carry

    lax.fori_loop(*OTHERS, rows_came, 0)
    phase("home")
    for j in range(NZ):
        home[j, :BACK, :] = ret[j]
    flat = home[...].reshape(NZ * SENT, LANES)
    out_tok[...] = dot(pall[...], flat, (0, 0)).astype(BF16)
    at_j = lax.broadcasted_iota(jnp.int32, (NZ, NZ * SENT), 0)
    at_row = lax.broadcasted_iota(jnp.int32, (NZ, NZ * SENT), 1)
    lines = dot((at_row == SENT * at_j + CAP).astype(F32).astype(BF16), flat, (1, 0))
    values = jnp.zeros((NZ, LANES), F32)
    lanes_of = lax.broadcasted_iota(jnp.int32, (NZ, LANES), 1)
    by_slot = jnp.zeros((NZ, PAD), F32)
    for i in range(LANES // PAD):
        mine = lax.broadcasted_iota(jnp.int32, (NZ, PAD), 0) % (LANES // PAD) == i
        by_slot = by_slot + jnp.where(mine, lines[:, PAD * i : PAD * (i + 1)], 0.0)
    by_slot = by_slot.astype(BF16)
    for j in range(NZ):
        mine = dot(by_slot, pall[SENT * j : SENT * j + PAD, :], (1, 0))
        values = jnp.where(lax.broadcasted_iota(jnp.int32, (NZ, LANES), 0) == j, mine, values)
    for i, hit in enumerate((hit0, hit1)):
        out_route[i : i + 1, :] = (
            jnp.sum(jnp.where(hit, values, 0.0), axis=0, keepdims=True) / weights[i : i + 1, :]
        )

    phase("drain")
    def drain(j, carry):
        to_expert(j).wait_send()
        home_of(j).wait_send()
        return carry

    lax.fori_loop(*OTHERS, drain, 0)
    for copy in waits:
        copy.wait_send()
    phase(None)


def store(*refs):
    n = len(refs) // 2
    copies = [
        pltpu.make_async_copy(refs[i], refs[n + i], refs[-1].at[i]) for i in range(n)
    ]
    for copy in copies:
        copy.start()
    for copy in copies:
        copy.wait()


def local(tokens, routes, route_weights, out_grad, gate_proj, up_proj, down_proj):
    vmem, hbm = pl.BlockSpec(memory_space=pltpu.VMEM), pl.BlockSpec(memory_space=pl.ANY)
    dma, buf = pltpu.SemaphoreType.DMA, pltpu.VMEM
    quad = (SIDE, HALF, LANES)
    shapes = [
        ((LANES, LANES), BF16),
        ((2, LANES), F32),
        ((1, MODEL, LANES), BF16),
        ((1, MODEL, LANES), BF16),
        ((1, LANES, MODEL), BF16),
    ]
    out = pl.pallas_call(
        kernel,
        out_shape=tuple(pltpu.VMEM(*s) for s in shapes),
        in_specs=[hbm] * 7,
        out_specs=[vmem] * 5,
        scratch_shapes=[
            buf((2, LANES), jnp.int32),
            buf((2, LANES), F32),
            buf((LANES, LANES), BF16),
            buf((LANES, LANES), BF16),
            buf((MODEL, 2 * LANES), BF16),
            buf((SIDE * SIDE, 2 * LANES, LANES), BF16),
            buf((LANES, MODEL), BF16),
            buf((MODEL, LANES), BF16),
            buf((NZ * SENT, LANES), BF16),
            buf((NZ * SENT, LANES), BF16),
            buf((NZ * SENT, LANES), BF16),
            buf((NZ * SENT, LANES), BF16),
            buf((2, ROWS, MODEL), BF16),
            buf((ROWS, 2 * LANES), BF16),
            buf((ROWS, LANES), BF16),
            buf((CHUNKS, SIDE, *quad), BF16),
            buf((CHUNKS, SIDE, *quad), BF16),
            buf((CHUNKS, SIDE, *quad), F32),
            buf((CHUNKS, SIDE, *quad), BF16),
            buf((CHUNKS, 3, *quad), BF16),
            buf((CHUNKS, *quad), BF16),
            buf((CHUNKS, 3, HALF, LANES), BF16),
            buf((NZ, BACK, LANES), BF16),
            buf((NZ, BACK, LANES), BF16),
            buf((NZ, SENT, LANES), BF16),
            buf((CHUNKS, 8, LANES), F32),
            buf((CHUNKS, 8, LANES), F32),
            buf((CHUNKS, 8, LANES), F32),
            buf((CHUNKS, SIDE * SIDE - 1, 8, LANES), F32),
            buf((CHUNKS, 8, LANES), F32),
            dma((7,)),
            dma((NZ,)),
            dma((NZ,)),
            dma((CHUNKS, 4)),
            dma((CHUNKS, 4)),
            dma((CHUNKS, SIDE, 4)),
            dma((CHUNKS, SIDE, 4)),
            dma((CHUNKS, SIDE * SIDE)),
            dma((CHUNKS, SIDE * SIDE)),
            dma((CHUNKS, SIDE)),
            dma((CHUNKS, SIDE)),
            dma((CHUNKS, SIDE)),
            dma((CHUNKS, SIDE)),
            dma((CHUNKS, SIDE)),
            dma((CHUNKS, SIDE)),
            dma((NZ,)),
            dma((NZ,)),
            dma((CHUNKS,)),
            dma((CHUNKS,)),
            dma((CHUNKS, SIDE * SIDE - 1)),
            dma((CHUNKS, SIDE * SIDE - 1)),
        ],
        compiler_params=pltpu.CompilerParams(
            collective_id=0, has_side_effects=True, vmem_limit_bytes=56 * 2**20
        ),
        name="routed_backward",
    )(routes.T, route_weights.T, tokens, out_grad, gate_proj, up_proj, down_proj)
    out = pl.pallas_call(
        store,
        out_shape=tuple(jax.ShapeDtypeStruct(*s) for s in shapes),
        in_specs=[vmem] * 5,
        out_specs=[hbm] * 5,
        scratch_shapes=[dma((5,))],
        name="store",
    )(*(pltpu.with_memory_space_constraint(a, pltpu.VMEM) for a in out))
    return (out[0], out[1].T, out[2], out[3], out[4])


SCHEDULE = (
    "arrive0", "gather00", "gather10", "gather20", "gather30", "arrive1", "gather01", "gather40",
    "gather11", "gather50", "gather60", "gather21", "gather70", "gather31", "expert0", "gate00",
    "gather41", "dx_other0", "gate10", "gather51", "scatter10", "gather61", "gather71",
    "expert1", "gate01", "dx_other1", "gate11", "scatter20", "scatter11", "gate20", "scatter30",
    "scatter21", "gate21", "scatter31", "unit_grads0", "down_grads0",
)


def solution(mesh):
    placed = (
        P("ep", None),
        P("ep", None),
        P("ep", None),
        P("ep", None),
        P("ep", None, "tp"),
        P("ep", None, "tp"),
        P("ep", "tp", None),
    )
    return jax.shard_map(
        local,
        mesh=mesh,
        in_specs=placed,
        out_specs=(
            P("ep", "tp"),
            P("ep", None),
            P("ep", None, "tp"),
            P("ep", None, "tp"),
            P("ep", "tp", None),
        ),
        check_vma=False,
    )
```

time: 80.1 us -> 72.1 us (0.900)
  the two profiles are of different devices: /device:TPU:14 before, /device:TPU:1 now
where the time goes in v3:
time: 72.1 us; the launch traced here: 71.8 us
  Pallas kernels  71.2 us (99%)
    pallas_call x1, Pallas kernels, local(): pl.pallas_call(kernel, out_shape=tuple((pltpu.VMEM(*s) for s in shapes)),...  70 us

profile of v3, /device:TPU:1, one launch (start us, length us, event | category | flops | bytes accessed | tf_op | source)
XLA Modules:
  0.0 71.8 jit_solution(8766891594066937596)
XLA Ops:
  0.6 70.0 %routed_backward.1 = (bf16[128,128]{1,0:T(8,128)(2,1)S(1)}, f32[2,128]{1,0:T(2,128)S(1)}, bf16[1,2048,128]{2,1,0:T(8,128)(2,1)S(1)}, bf16[1,2048,128]{2,1,0:T(8,128)(2,1)S(1)}, bf16[1,128,2048]{2,1,0:T(8,128)(2,1)S(1)}) custom-call(s32[2,128]{1,0:T(2,128)} %bitcast.3, f32[2,128]{1,0:T(2,128)} %bitcast.4, bf16[128,2048]{1,0:T(8,128)(2,1)} %tok_hbm.1, ...), custom_call_target="tpu_custom_call" | custom-call | tf_op jit(solution)/shard_map/routed_backward/pallas_call | solution.py:500
  70.6 1.2 %store.1 = (bf16[128,128]{1,0:T(8,128)(2,1)}, f32[2,128]{1,0:T(2,128)}, bf16[1,2048,128]{2,1,0:T(8,128)(2,1)}, bf16[1,2048,128]{2,1,0:T(8,128)(2,1)}, bf16[1,128,2048]{2,1,0:T(8,128)(2,1)}) custom-call(bf16[128,128]{1,0:T(8,128)(2,1)S(1)} %get-tuple-element.15.refs_0_, f32[2,128]{1,0:T(2,128)S(1)} %get-tuple-element.16.refs_1_, ...), custom_call_target="tpu_custom_call" | custom-call | tf_op jit(solution)/shard_map/store/pallas_call | solution.py:563
